TPU v7x, 32 devices: a whole 2x2x4 slice. The times are simulated.
32 devices in a mesh: rep: 4 (over z), fs: 2 (over y), tp: 4 (over x, core).
Axes of the slice: x: 2, y: 2, z: 4, core: 2. Of those that a mesh axis runs over, the one named last changes fastest.
Arguments:
- inputs: bfloat16 [2560, 2048], P('rep', 'fs'), may hold values from -6 to 6
- gate_pre: bfloat16 [2560, 5632], P('rep', 'tp'), may hold values from -12 to 12
- up_pre: bfloat16 [2560, 5632], P('rep', 'tp'), may hold values from -6 to 6
- cotangent: bfloat16 [2560, 2048], P('rep'), may hold values from -6 to 6
- w_gate: bfloat16 [2048, 5632], P('fs', 'tp'), may hold values from -0.125 to 0.125
- w_up: bfloat16 [2048, 5632], P('fs', 'tp'), may hold values from -0.125 to 0.125
- w_down: bfloat16 [5632, 2048], P('tp', 'fs'), may hold values from -0.078125 to 0.078125
Outputs:
- grad_input: bfloat16 [2560, 2048], P('rep', 'fs')
- grad_gate: float32 [512, 4, 5632], P('fs', 'rep', 'tp')
- grad_up: float32 [512, 4, 5632], P('fs', 'rep', 'tp')
- grad_down: float32 [5632, 512, 4], P('tp', 'fs', 'rep')
- gate_norms: float32 [512, 4], P('fs', 'rep')
- up_norms: float32 [512, 4], P('fs', 'rep')
- down_norms: float32 [5632], P('tp')
All inputs are finite; a program needn't handle non-finite values.
Results may differ from a plain program's by a relative error of at most 0.02.
Values may be sent and summed in bfloat16 or wider, within the bound.
A program may use at most 64 MiB of HBM per device.

v0:
```python
import functools

import jax
import jax.numpy as jnp
from jax import lax
from jax.experimental import pallas as pl
from jax.experimental.pallas import tpu as pltpu
from jax.sharding import PartitionSpec as P

LANES = 128
F32 = jnp.float32
BF16 = jnp.bfloat16
MESH = pl.DeviceIdType.MESH
NT = (((1,), (1,)), ((), ()))


def on_device(inputs, gate_pre, up_pre, cotangent, w_gate, w_up, w_down):
    single = jnp.float32
    groups = lax.axis_size("rep")
    width = w_down.shape[1]
    own_cot = lax.dynamic_slice_in_dim(cotangent, lax.axis_index("fs") * width, width, 1)
    partial_grad = jnp.einsum("td,fd->tf", own_cot, w_down, preferred_element_type=single)
    hidden_grad = lax.psum(partial_grad.astype(jnp.bfloat16), "fs").astype(jnp.float32)
    gate = gate_pre.astype(single)
    upper = up_pre.astype(single)
    sigma = jax.nn.sigmoid(gate)
    active = gate * sigma
    hidden = (active * upper).astype(jnp.bfloat16)
    d_up = (hidden_grad * active).astype(jnp.bfloat16)
    d_gate = (hidden_grad * upper * sigma * (1.0 + gate * (1.0 - sigma))).astype(jnp.bfloat16)
    factor = float(inputs.shape[0] * groups) ** (-0.5)
    owned = width // groups
    hunits = w_gate.shape[1]
    gate_local = jnp.einsum("td,tf->df", inputs, d_gate, preferred_element_type=single) * factor
    gate_parts = lax.all_to_all(
        gate_local.reshape(owned, groups, hunits).astype(jnp.bfloat16),
        "rep",
        split_axis=1,
        concat_axis=1,
        tiled=True,
    ).astype(jnp.float32)
    grad_gate = jnp.sum(gate_parts, axis=1, keepdims=True)
    up_local = jnp.einsum("td,tf->df", inputs, d_up, preferred_element_type=single) * factor
    up_parts = lax.all_to_all(
        up_local.reshape(owned, groups, hunits).astype(jnp.bfloat16),
        "rep",
        split_axis=1,
        concat_axis=1,
        tiled=True,
    ).astype(jnp.float32)
    grad_up = jnp.sum(up_parts, axis=1, keepdims=True)
    down_local = jnp.einsum("tf,td->fd", hidden, own_cot, preferred_element_type=single) * factor
    down_parts = lax.all_to_all(
        down_local.reshape(hunits, owned, groups).astype(jnp.bfloat16),
        "rep",
        split_axis=2,
        concat_axis=2,
        tiled=True,
    ).astype(jnp.float32)
    grad_down = jnp.sum(down_parts, axis=2, keepdims=True)
    input_term = jnp.einsum("tf,df->td", d_gate, w_gate, preferred_element_type=single)
    input_term = input_term + jnp.einsum("tf,df->td", d_up, w_up, preferred_element_type=single)
    grad_input = lax.psum(input_term.astype(jnp.bfloat16), "tp")
    gate_norms, up_norms = lax.psum(
        (jnp.sum(grad_gate * grad_gate, axis=2), jnp.sum(grad_up * grad_up, axis=2)), "tp"
    )
    down_norms = lax.psum(jnp.sum(grad_down * grad_down, axis=(1, 2)), ("rep", "fs"))
    return (grad_input, grad_gate, grad_up, grad_down, gate_norms, up_norms, down_norms)


def line_kernel(
    sizes, x_hbm, gate_hbm, up_hbm, cot_hbm, wg_hbm, wu_hbm, wd_hbm,
    gi_ref, gate_out, up_out, down_out, gu_norm_ref, down_norm_ref,
    x_ref, gate_ref, up_ref, cot_ref, wg_ref, wu_ref, wd_ref,
    left, left_far, right, right_far, pg_own, pg_peer, ab, sb, bb, gi_acc, gi_own, gi_peer,
    squares, gu_own, gu_peer, dn_own, dn_peer,
    load_sem, y_send, y_recv, a_send, a_recv, b_send, b_recv, c_send, c_recv,
    r_send, r_recv, f_send, f_recv, l_send, l_recv, m_send, m_recv,
    gi_send, gi_recv, gg_send, gg_recv, gn_send, gn_recv, dn_send, dn_recv,
):
    n_fs, n_tp, factor = sizes
    tokens, width = x_ref.shape
    hunits = gate_ref.shape[1]
    blocks = hunits // LANES
    items = 3 * blocks
    owned = width // 4
    share = tokens // n_tp
    rep, fs, tp = lax.axis_index("rep"), lax.axis_index("fs"), lax.axis_index("tp")
    side = rep // 2
    mid, end = 1 + side, 3 * side
    far_mid, far_end = 2 - side, 3 - 3 * side
    at_end = rep == end
    partner = mid + end - rep
    fs_peer = 1 - fs

    loads = [
        pltpu.make_async_copy(cot_hbm.at[:, pl.ds(pl.multiple_of(fs * width, LANES), width)], cot_ref, load_sem.at[0]),
        pltpu.make_async_copy(wd_hbm, wd_ref, load_sem.at[1]),
        pltpu.make_async_copy(gate_hbm, gate_ref, load_sem.at[2]),
        pltpu.make_async_copy(up_hbm, up_ref, load_sem.at[3]),
        pltpu.make_async_copy(x_hbm, x_ref, load_sem.at[4]),
        pltpu.make_async_copy(wg_hbm, wg_ref, load_sem.at[5]),
        pltpu.make_async_copy(wu_hbm, wu_ref, load_sem.at[6]),
    ]
    for k in (0, 2, 3, 4, 1, 5, 6):
        loads[k].start()

    group = [(r, f) for r in range(4) for f in range(n_fs) if r or f]

    def in_group(step):
        return (lax.rem(rep + step[0], 4), lax.rem(fs + step[1], n_fs), tp)

    def in_tp(step):
        return (rep, fs, lax.rem(tp + step, n_tp))

    barrier = pltpu.get_barrier_semaphore()
    greeted = [in_group(s) for s in group] + [in_tp(s) for s in range(1, n_tp)]
    for other in greeted:
        pl.semaphore_signal(barrier, inc=1, device_id=other, device_id_type=MESH)
    pl.semaphore_wait(barrier, len(greeted))

    def remote(src, dst, send, recv, other):
        return pltpu.make_async_remote_copy(
            src_ref=src, dst_ref=dst, send_sem=send, recv_sem=recv, device_id=other, device_id_type=MESH
        )

    def y_copy(j):
        return remote(pg_own.at[j], pg_peer.at[j], y_send.at[j], y_recv.at[j], (rep, fs_peer, tp))

    def a_copy(t):
        return remote(ab.at[t], ab.at[t], a_send.at[t], a_recv.at[t], (partner, fs, tp))

    def b_copy(kind, t):
        src = ab.at[t, pl.ds(owned, 2 * owned)] if kind == 0 else sb.at[t - blocks]
        return remote(src, bb.at[t], b_send.at[t], b_recv.at[t], (far_mid, fs, tp))

    def c_copy(t):
        return remote(
            bb.at[t, pl.ds(owned, owned)], bb.at[t, pl.ds(0, owned)], c_send.at[t], c_recv.at[t], (partner, fs, tp)
        )

    half = tokens // n_fs
    own_half = pl.ds(pl.multiple_of(fs * half, 16), half)

    def r_copy(q):
        return remote(
            right.at[blocks + q, own_half], right_far.at[q, own_half], r_send.at[q], r_recv.at[q], (partner, fs, tp)
        )

    def f_copy(q):
        piece = right_far.at[q, own_half]
        return remote(piece, piece, f_send.at[q], f_recv.at[q], (rep, fs_peer, tp))

    piece_rows = 3 * owned // n_tp
    own_piece = pl.ds(pl.multiple_of(tp * piece_rows, 16), piece_rows)

    def l_copy():
        return remote(left.at[1, own_piece], left_far.at[own_piece], l_send.at[0], l_recv.at[0], (partner, fs, tp))

    def m_copy(step):
        piece = left_far.at[own_piece]
        return remote(piece, piece, m_send.at[step - 1], m_recv.at[step - 1], in_tp(step))

    def lanes(j):
        return pl.ds(pl.multiple_of(j * LANES, LANES), LANES)

    def rows_of(slot):
        return slice(slot * owned, (slot + 1) * owned)

    def term(kind, slot, t):
        return jnp.dot(left[kind, rows_of(slot), :], right[t], preferred_element_type=F32) * factor

    def long_term(slot, t):
        own = jnp.dot(left[1, rows_of(slot), :], right[t], preferred_element_type=F32)
        far = jnp.dot(left_far[rows_of(slot), :], right_far[t - blocks], preferred_element_type=F32)
        return (own + far) * factor

    def loop(first, last, body):
        def step(i, carry):
            body(i)
            return carry
        lax.fori_loop(first, last, step, 0)

    lead = min(2, blocks - 1)
    ahead = min(5, blocks)

    def spread(kind, source):
        for slot, owner in enumerate((mid, far_mid, far_end, end)):
            place = lax.broadcasted_iota(jnp.int32, (owned, width), 0) * 4 + owner
            pick = (place == lax.broadcasted_iota(jnp.int32, (owned, width), 1)).astype(F32).astype(BF16)
            left[kind, rows_of(slot), :] = lax.dot_general(
                pick, source[...], NT, preferred_element_type=F32
            ).astype(BF16)

    loads[0].wait()
    spread(0, cot_ref)
    loads[2].wait()
    loads[3].wait()
    squares[...] = jnp.zeros_like(squares)
    dn_own[...] = jnp.zeros_like(dn_own)
    gu_own[...] = jnp.zeros_like(gu_own)

    def send_down(t):
        for slot in range(3):
            ab[t, rows_of(slot), :] = term(0, slot, t).astype(BF16)
        a_copy(t).start()

    def hidden_of(j):
        g = gate_ref[:, lanes(j)].astype(F32)
        u = up_ref[:, lanes(j)].astype(F32)
        right[j] = (g * (1.0 / (1.0 + jnp.exp(-g))) * u).astype(BF16)

    def hidden_first(j):
        hidden_of(j)

        @pl.when(at_end)
        def _():
            send_down(j)

    loop(0, 1, hidden_first)
    loads[4].wait()
    spread(1, x_ref)

    @pl.when(at_end)
    def _():
        l_copy().start()

    loop(1, lead, hidden_first)

    loads[1].wait()

    def partial_of(j):
        rows = pl.ds(pl.multiple_of(j * LANES, LANES), LANES)
        pg_own[j] = lax.dot_general(cot_ref[...], wd_ref[rows, :], NT, preferred_element_type=F32).astype(BF16)

        @pl.when(jnp.logical_or(at_end, j < ahead))
        def _():
            y_copy(j).start()

    loop(0, blocks, partial_of)

    loop(lead, blocks, hidden_of)

    def grads_of(j):
        y_copy(j).wait_recv()
        g = gate_ref[:, lanes(j)].astype(F32)
        u = up_ref[:, lanes(j)].astype(F32)
        total = pg_own[j].astype(F32) + pg_peer[j].astype(F32)
        s = 1.0 / (1.0 + jnp.exp(-g))
        t = blocks + 2 * j
        right[t] = (total * u * s * (1.0 + g * (1.0 - s))).astype(BF16)
        right[t + 1] = (total * (g * s)).astype(BF16)

    def finish(kind, j, piece):
        if kind == 0:
            dn_own[0:1, lanes(j)] = jnp.sum(piece * piece, axis=0, keepdims=True)
            down_out[pl.ds(pl.multiple_of(j * LANES, LANES), LANES), 0, :] = piece.T
        else:
            squares[kind - 1] += piece * piece
            (gate_out if kind == 1 else up_out)[:, 0, lanes(j)] = piece

    def item(kind, j):
        return j if kind == 0 else blocks + 2 * j + kind - 1

    def down_on(t):
        a_copy(t).wait_recv()
        for slot in (1, 2):
            ab[t, rows_of(slot), :] = (ab[t, rows_of(slot), :].astype(F32) + term(0, slot, t)).astype(BF16)
        b_copy(0, t).start()

    def forward(j):
        for q in (2 * j, 2 * j + 1):
            r_copy(q).wait_recv()
            f_copy(q).start()

    def pair_on(j):
        for kind in (1, 2):
            t = item(kind, j)
            f_copy(t - blocks).wait_recv()
            for slot in (1, 2):
                sb[t - blocks, rows_of(slot - 1), :] = long_term(slot, t).astype(BF16)
            b_copy(kind, t).start()

    def settle(kind, j):
        t = item(kind, j)
        b_copy(kind, t).wait_recv()
        bb[t, owned:, :] = (bb[t, owned:, :].astype(F32) + term(min(kind, 1), 3, t)).astype(BF16)
        c_copy(t).start()
        if kind == 0:
            own = ab[t, :owned, :].astype(F32) + term(0, 0, t)
        else:
            own = long_term(0, t)
        finish(kind, j, own + bb[t, :owned, :].astype(F32))

    def last_hop(kind, j):
        t = item(kind, j)
        c_copy(t).wait_recv()
        finish(kind, j, bb[t, :owned, :].astype(F32) + term(min(kind, 1), 3, t))

    def through(action, j, with_down=True):
        action(1, j)
        action(2, j)
        if with_down:
            action(0, j + lead)

    def gi_term(j):
        t = blocks + 2 * j
        gi_acc[...] += lax.dot_general(right[t], wg_ref[:, lanes(j)], NT, preferred_element_type=F32) + lax.dot_general(
            right[t + 1], wu_ref[:, lanes(j)], NT, preferred_element_type=F32
        )

    def grads_and_term(j):
        grads_of(j)
        gi_term(j)

    gi_acc[...] = jnp.zeros_like(gi_acc)
    downs = blocks - lead
    early = blocks - ahead

    @pl.when(at_end)
    def _():
        def pair_out(j):
            grads_of(j)
            r_copy(2 * j).start()
            r_copy(2 * j + 1).start()

        def both_out(j):
            pair_out(j)
            send_down(j + lead)

        loop(0, downs, both_out)
        loop(downs, blocks, pair_out)
        loads[5].wait()
        loads[6].wait()
        loop(0, blocks, gi_term)

    @pl.when(jnp.logical_not(at_end))
    def _():
        loads[5].wait()
        loads[6].wait()
        down_on(0)
        l_copy().wait_recv()
        for step in range(1, n_tp):
            m_copy(step).start()
        loop(1, lead, down_on)
        forward(0)
        for step in range(1, n_tp):
            m_copy(step).wait_recv()
        grads_and_term(0)
        forward(1)
        y_copy(ahead).start()
        pair_on(0)
        down_on(lead)
        loop(0, lead, functools.partial(settle, 0))

        def step(j):
            grads_of(j)
            forward(j + 1)
            y_copy(ahead + j).start()
            pair_on(j)
            down_on(j + lead)
            gi_term(j)
            through(settle, j - 1)

            @pl.when(j > 1)
            def _():
                grads_and_term(ahead - 1 + j)

        loop(1, early, step)
        loop(ahead - 1 + early, blocks, grads_and_term)

    gi_own[...] = gi_acc[...].astype(BF16)

    def tokens_of(owner):
        return pl.ds(pl.multiple_of(owner * share, share), share)

    def gi_copy(step):
        other = lax.rem(tp + step, n_tp)
        return remote(
            gi_own.at[tokens_of(other)], gi_peer.at[step - 1], gi_send.at[step - 1], gi_recv.at[step - 1], in_tp(step)
        )

    def gg_copy(step):
        return remote(
            gi_ref.at[tokens_of(tp)], gi_ref.at[tokens_of(tp)], gg_send.at[step - 1], gg_recv.at[step - 1], in_tp(step)
        )

    for step in range(1, n_tp):
        gi_copy(step).start()

    @pl.when(at_end)
    def _():
        loop(0, lead, functools.partial(last_hop, 0))
        loop(0, downs, functools.partial(through, last_hop))

    @pl.when(jnp.logical_not(at_end))
    def _():
        def step(j):
            forward(j + 1)
            pair_on(j)
            down_on(j + lead)
            through(settle, j - 1)

        loop(early, downs, step)
        forward(downs + 1)
        pair_on(downs)
        through(settle, downs - 1)

    def dn_copy(k):
        return remote(dn_own, dn_peer.at[k], dn_send.at[k], dn_recv.at[k], in_group(group[k]))

    for k in range(len(group)):
        dn_copy(k).start()

    for step in range(1, n_tp):
        gi_copy(step).wait_recv()
    whole = gi_own[tokens_of(tp), :].astype(F32)
    for step in range(1, n_tp):
        whole += gi_peer[step - 1].astype(F32)
    gi_ref[tokens_of(tp), :] = whole.astype(BF16)
    for step in range(1, n_tp):
        gg_copy(step).start()

    @pl.when(at_end)
    def _():
        loop(downs, blocks, functools.partial(through, last_hop, with_down=False))

    @pl.when(jnp.logical_not(at_end))
    def _():
        def step(j):
            forward(j + 1)
            pair_on(j)
            through(settle, j - 1, with_down=False)

        loop(downs + 1, blocks - 1, step)
        pair_on(blocks - 1)
        through(settle, blocks - 2, with_down=False)
        through(settle, blocks - 1, with_down=False)

    for kind in range(2):
        gu_own[kind:kind + 1, :] = jnp.sum(squares[kind].T, axis=0, keepdims=True)

    def gn_copy(step):
        return remote(gu_own, gu_peer.at[step - 1], gn_send.at[step - 1], gn_recv.at[step - 1], in_tp(step))

    for step in range(1, n_tp):
        gn_copy(step).start()

    for k in range(len(group)):
        dn_copy(k).wait_recv()
    down = dn_own[...]
    for k in range(len(group)):
        down += dn_peer[k]
    down_norm_ref[...] = down

    for step in range(1, n_tp):
        gn_copy(step).wait_recv()
    gate_up = gu_own[...]
    for step in range(1, n_tp):
        gate_up += gu_peer[step - 1]
    gu_norm_ref[...] = gate_up

    for step in range(1, n_tp):
        gg_copy(step).wait_recv()
        gg_copy(step).wait_send()
        gi_copy(step).wait_send()
        gn_copy(step).wait_send()
    for k in range(len(group)):
        dn_copy(k).wait_send()
    loop(0, blocks, lambda j: y_copy(j).wait_send())

    @pl.when(at_end)
    def _():
        l_copy().wait_send()
        loop(0, blocks, lambda t: a_copy(t).wait_send())
        loop(0, 2 * blocks, lambda q: r_copy(q).wait_send())

    @pl.when(jnp.logical_not(at_end))
    def _():
        for step in range(1, n_tp):
            m_copy(step).wait_send()
        loop(0, blocks, lambda t: b_copy(0, t).wait_send())
        loop(blocks, items, lambda t: b_copy(1, t).wait_send())
        loop(0, items, lambda t: c_copy(t).wait_send())
        loop(0, 2 * blocks, lambda q: f_copy(q).wait_send())


def on_line(inputs, gate_pre, up_pre, cotangent, w_gate, w_up, w_down):
    n_fs, n_tp = lax.axis_size("fs"), lax.axis_size("tp")
    tokens, width = inputs.shape
    hunits = w_gate.shape[1]
    blocks = hunits // LANES
    items = 3 * blocks
    owned = width // 4
    share = tokens // n_tp
    n_group = 4 * n_fs - 1
    dma = pltpu.SemaphoreType.DMA
    vmem = pltpu.VMEM
    sizes = (n_fs, n_tp, float(tokens * 4) ** (-0.5))
    grad_input, grad_gate, grad_up, grad_down, gate_up, down = pl.pallas_call(
        functools.partial(line_kernel, sizes),
        out_shape=(
            jax.ShapeDtypeStruct((tokens, width), BF16),
            jax.ShapeDtypeStruct((owned, 1, hunits), F32),
            jax.ShapeDtypeStruct((owned, 1, hunits), F32),
            jax.ShapeDtypeStruct((hunits, 1, owned), F32),
            jax.ShapeDtypeStruct((8, owned), F32),
            jax.ShapeDtypeStruct((8, hunits), F32),
        ),
        in_specs=[pl.BlockSpec(memory_space=pl.ANY)] * 7,
        out_specs=(pl.BlockSpec(memory_space=vmem),) * 6,
        scratch_shapes=[
            vmem((tokens, width), BF16),
            vmem((tokens, hunits), BF16),
            vmem((tokens, hunits), BF16),
            vmem((tokens, width), BF16),
            vmem((width, hunits), BF16),
            vmem((width, hunits), BF16),
            vmem((hunits, width), BF16),
            vmem((2, width, tokens), BF16),
            vmem((3 * owned, tokens), BF16),
            vmem((items, tokens, LANES), BF16),
            vmem((2 * blocks, tokens, LANES), BF16),
            vmem((blocks, tokens, LANES), BF16),
            vmem((blocks, tokens, LANES), BF16),
            vmem((blocks, 3 * owned, LANES), BF16),
            vmem((2 * blocks, 2 * owned, LANES), BF16),
            vmem((items, 2 * owned, LANES), BF16),
            vmem((tokens, width), F32),
            vmem((tokens, width), BF16),
            vmem((n_tp - 1, share, width), BF16),
            vmem((2, owned, LANES), F32),
            vmem((8, owned), F32),
            vmem((n_tp - 1, 8, owned), F32),
            vmem((8, hunits), F32),
            vmem((n_group, 8, hunits), F32),
            dma((7,)),
            dma((blocks,)), dma((blocks,)),
            dma((blocks,)), dma((blocks,)),
            dma((items,)), dma((items,)),
            dma((items,)), dma((items,)),
            dma((2 * blocks,)), dma((2 * blocks,)),
            dma((2 * blocks,)), dma((2 * blocks,)),
            dma((1,)), dma((1,)),
            dma((n_tp - 1,)), dma((n_tp - 1,)),
            dma((n_tp - 1,)), dma((n_tp - 1,)),
            dma((n_tp - 1,)), dma((n_tp - 1,)),
            dma((n_tp - 1,)), dma((n_tp - 1,)),
            dma((n_group,)), dma((n_group,)),
        ],
        compiler_params=pltpu.CompilerParams(
            collective_id=0, has_side_effects=True, vmem_limit_bytes=67043328
        ),
    )(inputs, gate_pre, up_pre, cotangent, w_gate, w_up, w_down)
    return (
        grad_input,
        grad_gate,
        grad_up,
        grad_down.transpose(0, 2, 1),
        gate_up[0].reshape(owned, 1),
        gate_up[1].reshape(owned, 1),
        down[0],
    )


def fits_line(mesh, inputs, w_gate):
    n_rep, n_fs, n_tp = (mesh.shape[axis] for axis in ("rep", "fs", "tp"))
    tokens, width = inputs.shape[0] // n_rep, inputs.shape[1] // n_fs
    return (
        n_rep == 4 and n_fs == 2 and n_tp > 1 and w_gate.shape[1] // n_tp >= 10 * LANES
        and (3 * width // 4) % (16 * n_tp) == 0
        and tokens % (16 * n_tp) == 0 and tokens % LANES == 0
        and width % (4 * LANES) == 0 and (w_gate.shape[1] // n_tp) % LANES == 0
    )


def solution(mesh):
    placed = (
        P("rep", "fs"),
        P("rep", "tp"),
        P("rep", "tp"),
        P("rep", None),
        P("fs", "tp"),
        P("fs", "tp"),
        P("tp", "fs"),
    )
    out_placed = (
        P("rep", "fs"),
        P("fs", "rep", "tp"),
        P("fs", "rep", "tp"),
        P("tp", "fs", "rep"),
        P("fs", "rep"),
        P("fs", "rep"),
        P("tp"),
    )

    def whole(inputs, gate_pre, up_pre, cotangent, w_gate, w_up, w_down):
        body = on_line if fits_line(mesh, inputs, w_gate) else on_device
        mapped = jax.shard_map(body, mesh=mesh, in_specs=placed, out_specs=out_placed, check_vma=False)
        return mapped(inputs, gate_pre, up_pre, cotangent, w_gate, w_up, w_down)

    return whole
```

profile of v0, /device:TPU:0, one launch (start us, length us, event | category | flops | bytes accessed | tf_op | source)
XLA Modules:
  0.0 153.1 jit_solution(9924382792280325902)
XLA Ops:
  0.6 142.3 %shard_map.126 = (bf16[640,1024]{1,0:T(8,128)(2,1)}, f32[256,1,1408]{2,1,0:T(1,128)}, f32[256,1,1408]{2,1,0:T(1,128)}, f32[1408,1,256]{2,1,0:T(1,128)}, f32[8,256]{1,0:T(8,128)}, /*index=5*/f32[8,1408]{1,0:T(8,128)}) custom-call(bf16[640,1024]{1,0:T(8,128)(2,1)} %x_hbm.1, bf16[640,1408]{1,0:T(8,128)(2,1)} %gate_hbm.1, bf16[640,1408]{1,0:T(8,128)(2,1)} %up_hbm.1, ...), custom_call_target="tpu_custom_call" | custom-call | tf_op jit(solution)/shard_map/pallas_call | solution.py:500
  143.0 0.0 copy-start.2
  143.0 1.4 slice_bitcast_fusion
  144.4 1.4 slice_reduce_fusion
  145.8 2.5 %copy.18 = bf16[640,1024]{1,0:T(8,128)(2,1)} copy(bf16[640,1024]{1,0:T(8,128)(2,1)} %get-tuple-element.28) | data formatting | bytes 2621440
  148.3 0.0 copy-done.2
  148.3 0.0 copy-start.1
  148.3 1.1 copy.19
  149.4 0.8 copy-done.1
  150.2 0.0 copy-start
  150.2 1.1 copy.20
  151.3 0.8 copy-done
  152.0 1.1 copy.21
Async XLA Ops:
  143.0 5.3 %copy-start.2 = (f32[256,1,1408]{2,1,0:T(1,128)S(1)}, f32[256,1,1408]{2,1,0:T(1,128)}, u32[]{:S(2)}) copy-start(f32[256,1,1408]{2,1,0:T(1,128)} %get-tuple-element.29) | copy-start | bytes 4325380
  148.3 1.9 %copy-start.1 = (f32[256,1,1408]{2,1,0:T(1,128)S(1)}, f32[256,1,1408]{2,1,0:T(1,128)}, u32[]{:S(2)}) copy-start(f32[256,1,1408]{2,1,0:T(1,128)} %get-tuple-element.30) | copy-start | bytes 4325380
  150.2 1.9 %copy-start = (f32[1408,1,256]{2,1,0:T(1,128)S(1)}, f32[1408,1,256]{2,1,0:T(1,128)}, u32[]{:S(2)}) copy-start(f32[1408,1,256]{2,1,0:T(1,128)} %get-tuple-element.16) | copy-start | bytes 4325380
where the time goes:
time: 153 us
  Pallas kernels  142 us (93%)
  local copies, waits for them, and re-layouts  10.1 us (7%)
    pallas_call x1, Pallas kernels, on_line(): pl.pallas_call(functools.partial(line_kernel, sizes), out_shape=(jax.Shap...  142 us
    unnamed x10, local copies, waits for them, and re-layouts  7.33 us

commit v1 on v0

v1 whole, which is shorter than its diff:
```python
import functools

import jax
import jax.numpy as jnp
from jax import lax
from jax.experimental import pallas as pl
from jax.experimental.pallas import tpu as pltpu
from jax.sharding import PartitionSpec as P

LANES = 128
CHUNK = 256
LATE = 4
VMEM_LIMIT = 56 * 2**20
F32 = jnp.float32
BF16 = jnp.bfloat16
MESH = pl.DeviceIdType.MESH
NT = (((1,), (1,)), ((), ()))


def on_device(inputs, gate_pre, up_pre, cotangent, w_gate, w_up, w_down):
    single = jnp.float32
    groups = lax.axis_size("rep")
    width = w_down.shape[1]
    own_cot = lax.dynamic_slice_in_dim(cotangent, lax.axis_index("fs") * width, width, 1)
    partial_grad = jnp.einsum("td,fd->tf", own_cot, w_down, preferred_element_type=single)
    hidden_grad = lax.psum(partial_grad.astype(jnp.bfloat16), "fs").astype(jnp.float32)
    gate = gate_pre.astype(single)
    upper = up_pre.astype(single)
    sigma = jax.nn.sigmoid(gate)
    active = gate * sigma
    hidden = (active * upper).astype(jnp.bfloat16)
    d_up = (hidden_grad * active).astype(jnp.bfloat16)
    d_gate = (hidden_grad * upper * sigma * (1.0 + gate * (1.0 - sigma))).astype(jnp.bfloat16)
    factor = float(inputs.shape[0] * groups) ** (-0.5)
    owned = width // groups
    hunits = w_gate.shape[1]
    gate_local = jnp.einsum("td,tf->df", inputs, d_gate, preferred_element_type=single) * factor
    gate_parts = lax.all_to_all(
        gate_local.reshape(owned, groups, hunits).astype(jnp.bfloat16),
        "rep",
        split_axis=1,
        concat_axis=1,
        tiled=True,
    ).astype(jnp.float32)
    grad_gate = jnp.sum(gate_parts, axis=1, keepdims=True)
    up_local = jnp.einsum("td,tf->df", inputs, d_up, preferred_element_type=single) * factor
    up_parts = lax.all_to_all(
        up_local.reshape(owned, groups, hunits).astype(jnp.bfloat16),
        "rep",
        split_axis=1,
        concat_axis=1,
        tiled=True,
    ).astype(jnp.float32)
    grad_up = jnp.sum(up_parts, axis=1, keepdims=True)
    down_local = jnp.einsum("tf,td->fd", hidden, own_cot, preferred_element_type=single) * factor
    down_parts = lax.all_to_all(
        down_local.reshape(hunits, owned, groups).astype(jnp.bfloat16),
        "rep",
        split_axis=2,
        concat_axis=2,
        tiled=True,
    ).astype(jnp.float32)
    grad_down = jnp.sum(down_parts, axis=2, keepdims=True)
    input_term = jnp.einsum("tf,df->td", d_gate, w_gate, preferred_element_type=single)
    input_term = input_term + jnp.einsum("tf,df->td", d_up, w_up, preferred_element_type=single)
    grad_input = lax.psum(input_term.astype(jnp.bfloat16), "tp")
    gate_norms, up_norms = lax.psum(
        (jnp.sum(grad_gate * grad_gate, axis=2), jnp.sum(grad_up * grad_up, axis=2)), "tp"
    )
    down_norms = lax.psum(jnp.sum(grad_down * grad_down, axis=(1, 2)), ("rep", "fs"))
    return (grad_input, grad_gate, grad_up, grad_down, gate_norms, up_norms, down_norms)


def line_kernel(
    sizes, x_hbm, gate_hbm, up_hbm, cot_hbm, wg_hbm, wu_hbm, wd_hbm,
    gi_ref, gate_out, up_out, down_out, gu_norm_ref, down_norm_ref,
    x_ref, gate_ref, up_ref, cot_ref, wg_ref, wu_ref, wd_ref,
    left, left_far, right, right_far, pg_own, pg_peer, ab, sb, bb, gi_acc, gi_own, gi_peer,
    squares, gu_own, gu_peer, dn_own, dn_peer,
    load_sem, y_send, y_recv, a_send, a_recv, b_send, b_recv, c_send, c_recv,
    r_send, r_recv, f_send, f_recv, l_send, l_recv, m_send, m_recv,
    gi_send, gi_recv, gg_send, gg_recv, gn_send, gn_recv, dn_send, dn_recv,
):
    n_fs, n_tp, factor = sizes
    tokens, width = x_ref.shape
    hunits = gate_ref.shape[1]
    blocks = hunits // LANES
    owned = width // 4
    share = tokens // n_tp
    rep, fs, tp = lax.axis_index("rep"), lax.axis_index("fs"), lax.axis_index("tp")
    side = rep // 2
    mid, end = 1 + side, 3 * side
    far_mid, far_end = 2 - side, 3 - 3 * side
    at_end = rep == end
    partner = mid + end - rep
    fs_peer = 1 - fs
    tp_next = tp + 1 - 2 * lax.rem(tp, 2)
    tp_far = lax.rem(tp + 2, n_tp)

    loads = [
        pltpu.make_async_copy(cot_hbm.at[:, pl.ds(pl.multiple_of(fs * width, LANES), width)], cot_ref, load_sem.at[0]),
        pltpu.make_async_copy(wd_hbm, wd_ref, load_sem.at[1]),
        pltpu.make_async_copy(gate_hbm, gate_ref, load_sem.at[2]),
        pltpu.make_async_copy(up_hbm, up_ref, load_sem.at[3]),
        pltpu.make_async_copy(x_hbm, x_ref, load_sem.at[4]),
        pltpu.make_async_copy(wg_hbm, wg_ref, load_sem.at[5]),
        pltpu.make_async_copy(wu_hbm, wu_ref, load_sem.at[6]),
    ]
    for k in (4, 0, 1, 2, 3, 5, 6):
        loads[k].start()

    group = [(r, f) for r in range(4) for f in range(n_fs) if r or f]

    def in_group(step):
        return (lax.rem(rep + step[0], 4), lax.rem(fs + step[1], n_fs), tp)

    def in_tp(step):
        return (rep, fs, lax.rem(tp + step, n_tp))

    barrier = pltpu.get_barrier_semaphore()
    greeted = [in_group(s) for s in group] + [in_tp(s) for s in range(1, n_tp)]
    for other in greeted:
        pl.semaphore_signal(barrier, inc=1, device_id=other, device_id_type=MESH)

    def remote(src, dst, send, recv, other):
        return pltpu.make_async_remote_copy(
            src_ref=src, dst_ref=dst, send_sem=send, recv_sem=recv, device_id=other, device_id_type=MESH
        )

    def rows_of(slot):
        return slice(slot * owned, (slot + 1) * owned)

    def y_copy(j):
        return remote(pg_own.at[j], pg_peer.at[j], y_send.at[j], y_recv.at[j], (rep, fs_peer, tp))

    def a_copy(t, late):
        piece = ab.at[t, pl.ds(0, owned) if late else pl.ds(owned, 2 * owned)]
        k = blocks * late + t
        return remote(piece, piece, a_send.at[k], a_recv.at[k], (partner, fs, tp))

    def b_copy(kind, t):
        src = ab.at[t, pl.ds(owned, 2 * owned)] if kind == 0 else sb.at[t - blocks]
        return remote(src, bb.at[t], b_send.at[t], b_recv.at[t], (far_mid, fs, tp))

    def c_copy(t):
        return remote(
            bb.at[t, pl.ds(owned, owned)], bb.at[t, pl.ds(0, owned)], c_send.at[t], c_recv.at[t], (partner, fs, tp)
        )

    half = tokens // n_fs
    own_half = pl.ds(pl.multiple_of(fs * half, 16), half)

    def r_copy(q):
        return remote(
            right.at[blocks + q, own_half], right_far.at[q, own_half], r_send.at[q], r_recv.at[q], (partner, fs, tp)
        )

    def f_copy(q):
        piece = right_far.at[q, own_half]
        return remote(piece, piece, f_send.at[q], f_recv.at[q], (rep, fs_peer, tp))

    piece_rows = owned // n_tp

    def piece_of(slot, owner):
        return pl.ds(pl.multiple_of(slot * owned + owner * piece_rows, 16), piece_rows)

    def l_copy(slot):
        rows = piece_of(slot, tp)
        return remote(left.at[1, rows], left_far.at[rows], l_send.at[slot], l_recv.at[slot], (partner, fs, tp))

    def m_copy(slot, hop):
        piece = left_far.at[piece_of(slot, tp_far if hop == 2 else tp)]
        k = 3 * slot + hop
        return remote(piece, piece, m_send.at[k], m_recv.at[k], (rep, fs, tp_next if hop else tp_far))

    def lanes(j):
        return pl.ds(pl.multiple_of(j * LANES, LANES), LANES)

    def term(kind, first, last, t):
        rows = slice(first * owned, last * owned)
        return jnp.dot(left[kind, rows, :], right[t], preferred_element_type=F32) * factor

    def long_term(first, last, t):
        rows = slice(first * owned, last * owned)
        own = jnp.dot(left[1, rows, :], right[t], preferred_element_type=F32)
        far = jnp.dot(left_far[rows, :], right_far[t - blocks], preferred_element_type=F32)
        return (own + far) * factor

    def loop(first, last, body):
        def step(i, carry):
            body(i)
            return carry
        lax.fori_loop(first, last, step, 0)

    def spread(kind, source):
        rows = CHUNK // 4
        lane = lax.broadcasted_iota(jnp.int32, (rows, CHUNK), 1)
        place = lax.broadcasted_iota(jnp.int32, (rows, CHUNK), 0) * 4
        pick = jnp.concatenate(
            [(place + owner == lane).astype(F32).astype(BF16) for owner in (mid, far_mid, far_end, end)], axis=0
        )
        for c in range(width // CHUNK):
            picked = lax.dot_general(
                pick, source[:, c * CHUNK:(c + 1) * CHUNK], NT, preferred_element_type=F32
            ).astype(BF16)
            for slot in range(4):
                left[kind, slot * owned + c * rows:slot * owned + (c + 1) * rows, :] = picked[slot * rows:(slot + 1) * rows]

    def item(kind, j):
        return j if kind == 0 else blocks + 2 * j + kind - 1

    def hidden_of(j):
        g = gate_ref[:, lanes(j)].astype(F32)
        u = up_ref[:, lanes(j)].astype(F32)
        right[j] = (g * (1.0 / (1.0 + jnp.exp(-g))) * u).astype(BF16)

    def send_down(t):
        ab[t] = term(0, 0, 3, t).astype(BF16)
        a_copy(t, 0).start()

    def partial_of(j):
        rows = pl.ds(pl.multiple_of(j * LANES, LANES), LANES)
        pg_own[j] = lax.dot_general(cot_ref[...], wd_ref[rows, :], NT, preferred_element_type=F32).astype(BF16)

    def partial_out(j):
        partial_of(j)
        y_copy(j).start()

    def grads_of(j):
        y_copy(j).wait_recv()
        g = gate_ref[:, lanes(j)].astype(F32)
        u = up_ref[:, lanes(j)].astype(F32)
        total = pg_own[j].astype(F32) + pg_peer[j].astype(F32)
        s = 1.0 / (1.0 + jnp.exp(-g))
        t = blocks + 2 * j
        right[t] = (total * u * s * (1.0 + g * (1.0 - s))).astype(BF16)
        right[t + 1] = (total * (g * s)).astype(BF16)

    def finish(kind, j, piece):
        if kind == 0:
            dn_own[0:1, lanes(j)] = jnp.sum(piece * piece, axis=0, keepdims=True)
            down_out[pl.ds(pl.multiple_of(j * LANES, LANES), LANES), 0, :] = piece.T
        else:
            squares[kind - 1] += piece * piece
            (gate_out if kind == 1 else up_out)[:, 0, lanes(j)] = piece

    def down_on(t):
        a_copy(t, 0).wait_recv()
        rows = slice(owned, 3 * owned)
        ab[t, rows, :] = (ab[t, rows, :].astype(F32) + term(0, 1, 3, t)).astype(BF16)
        b_copy(0, t).start()

    def forward(q):
        r_copy(q).wait_recv()
        f_copy(q).start()

    def pair_on(kind, j):
        t = item(kind, j)
        f_copy(t - blocks).wait_recv()
        sb[t - blocks] = long_term(1, 3, t).astype(BF16)
        b_copy(kind, t).start()

    def settle(kind, j):
        t = item(kind, j)
        b_copy(kind, t).wait_recv()
        bb[t, owned:, :] = (bb[t, owned:, :].astype(F32) + term(min(kind, 1), 3, 4, t)).astype(BF16)
        c_copy(t).start()
        if kind:
            finish(kind, j, long_term(0, 1, t) + bb[t, :owned, :].astype(F32))

    def settle_own(j):
        a_copy(j, 1).wait_recv()
        finish(0, j, ab[j, :owned, :].astype(F32) + term(0, 0, 1, j) + bb[j, :owned, :].astype(F32))

    def last_hop(kind, j):
        t = item(kind, j)
        c_copy(t).wait_recv()
        finish(kind, j, bb[t, :owned, :].astype(F32) + term(min(kind, 1), 3, 4, t))

    def gi_term(j):
        t = blocks + 2 * j
        gi_acc[...] += lax.dot_general(right[t], wg_ref[:, lanes(j)], NT, preferred_element_type=F32) + lax.dot_general(
            right[t + 1], wu_ref[:, lanes(j)], NT, preferred_element_type=F32
        )

    def grads_and_term(j):
        grads_of(j)
        gi_term(j)

    def tokens_of(owner):
        return pl.ds(pl.multiple_of(owner * share, share), share)

    def gi_copy(step):
        other = lax.rem(tp + step, n_tp)
        return remote(
            gi_own.at[tokens_of(other)], gi_peer.at[step - 1], gi_send.at[step - 1], gi_recv.at[step - 1], in_tp(step)
        )

    def gg_copy(hop):
        piece = gi_ref.at[tokens_of(tp_far if hop == 2 else tp)]
        return remote(piece, piece, gg_send.at[hop], gg_recv.at[hop], (rep, fs, tp_next if hop else tp_far))

    def gi_out():
        gi_own[...] = gi_acc[...].astype(BF16)
        for step in range(1, n_tp):
            gi_copy(step).start()

    def gi_sum():
        for step in range(1, n_tp):
            gi_copy(step).wait_recv()
        whole = gi_own[tokens_of(tp), :].astype(F32)
        for step in range(1, n_tp):
            whole += gi_peer[step - 1].astype(F32)
        gi_ref[tokens_of(tp), :] = whole.astype(BF16)
        gg_copy(0).start()
        gg_copy(1).start()

    def gi_pass():
        gg_copy(0).wait_recv()
        gg_copy(2).start()

    def dn_copy(k):
        return remote(dn_own, dn_peer.at[k], dn_send.at[k], dn_recv.at[k], in_group(group[k]))

    def dn_out():
        for k in range(len(group)):
            dn_copy(k).start()

    def gn_copy(step):
        return remote(gu_own, gu_peer.at[step - 1], gn_send.at[step - 1], gn_recv.at[step - 1], in_tp(step))

    loads[4].wait()
    spread(1, x_ref)
    pl.semaphore_wait(barrier, len(greeted))

    @pl.when(at_end)
    def _():
        l_copy(1).start()
        l_copy(2).start()

    loads[0].wait()
    loads[1].wait()
    loop(0, 1, partial_out)
    spread(0, cot_ref)
    loads[2].wait()
    loads[3].wait()

    @pl.when(at_end)
    def _():
        def out(j):
            hidden_of(j)
            send_down(j)

        def pair_out(j):
            grads_of(j)
            r_copy(2 * j).start()
            r_copy(2 * j + 1).start()

        loop(0, 1, out)
        loop(1, 6, partial_out)
        gi_acc[...] = jnp.zeros_like(gi_acc)

        def both_out(j):
            pair_out(j)
            out(j + 1)

            @pl.when(j == 1)
            def _():
                l_copy(0).start()

            @pl.when(j >= LATE)
            def _():
                a_copy(j - LATE, 1).start()

        loop(0, 1, both_out)
        loop(6, blocks, partial_out)
        loop(1, blocks - 1, both_out)
        pair_out(blocks - 1)
        loop(blocks - 1 - LATE, blocks, lambda t: a_copy(t, 1).start())
        squares[...] = jnp.zeros_like(squares)
        loads[5].wait()
        loads[6].wait()
        loop(0, blocks, gi_term)
        gi_out()

        def hops(j):
            last_hop(0, j - 1)
            last_hop(1, j - 2)
            last_hop(2, j - 2)

        last_hop(0, 0)
        loop(2, blocks - 3, hops)
        gi_sum()
        loop(blocks - 3, blocks, hops)
        last_hop(0, blocks - 1)
        dn_out()
        gi_pass()
        for j in (blocks - 2, blocks - 1):
            last_hop(1, j)
            last_hop(2, j)

    @pl.when(jnp.logical_not(at_end))
    def _():
        loop(1, 2, partial_out)
        loop(2, 6, partial_of)
        for slot in (1, 2):
            l_copy(slot).wait_recv()
            m_copy(slot, 0).start()
            m_copy(slot, 1).start()
        loop(6, blocks, partial_of)
        loop(0, blocks, hidden_of)
        down_on(0)
        grads_of(0)
        for slot in (1, 2):
            m_copy(slot, 0).wait_recv()
            m_copy(slot, 2).start()
        forward(0)
        gi_acc[...] = jnp.zeros_like(gi_acc)
        squares[...] = jnp.zeros_like(squares)
        loads[5].wait()
        loads[6].wait()
        forward(1)
        y_copy(2).start()
        for slot in (1, 2):
            m_copy(slot, 1).wait_recv()
            m_copy(slot, 2).wait_recv()
        pair_on(1, 0)
        down_on(1)
        pair_on(2, 0)
        grads_and_term(1)

        def first_y(j):
            return j + 2 + jnp.where(j > 3, 1, 0) + jnp.where(j > 5, 1, 0)

        def step(j, late):
            forward(2 * j)
            forward(2 * j + 1)
            if not late:
                new, old = first_y(j), first_y(j - 1)
                for extra in range(2):
                    @pl.when(jnp.logical_and(new + extra < blocks, extra == 0 if extra == 0 else jnp.logical_or(j == 3, j == 5)))
                    def _():
                        y_copy(new + extra).start()
                for extra in range(2):
                    @pl.when(jnp.logical_and(old + extra < blocks, extra == 0 if extra == 0 else jnp.logical_or(j == 4, j == 6)))
                    def _():
                        grads_and_term(old + extra)
            pair_on(1, j)
            pair_on(2, j)

        def early_step(j):
            step(j, False)
            down_on(j + 1)

        loop(1, 2, early_step)
        gi_term(0)
        l_copy(0).wait_recv()
        m_copy(0, 0).start()
        m_copy(0, 1).start()
        settle(0, 0)
        m_copy(0, 0).wait_recv()
        m_copy(0, 2).start()

        def settles(j):
            settle(0, j - 1)
            settle(1, j - 2)
            settle(2, j - 2)

            @pl.when(j >= LATE + 1)
            def _():
                settle_own(j - LATE - 1)

        loop(2, 3, early_step)
        m_copy(0, 1).wait_recv()
        m_copy(0, 2).wait_recv()

        def both(j):
            settles(j - 1)
            early_step(j)

        loop(3, blocks - 3, both)
        gi_out()

        def late_both(j):
            settles(j - 1)
            step(j, True)
            down_on(j + 1)

        loop(blocks - 3, blocks - 1, late_both)
        gi_sum()
        settles(blocks - 2)
        step(blocks - 1, True)
        settles(blocks - 1)
        gi_pass()
        loop(blocks - 1 - LATE, blocks - 1, settle_own)
        settle(0, blocks - 1)
        settle_own(blocks - 1)
        dn_out()
        for j in (blocks - 2, blocks - 1):
            settle(1, j)
            settle(2, j)

    for kind in range(2):
        gu_own[0:1, kind * owned:(kind + 1) * owned] = jnp.sum(squares[kind].T, axis=0, keepdims=True)
    for step in range(1, n_tp):
        gn_copy(step).start()

    for k in range(len(group)):
        dn_copy(k).wait_recv()
    down = dn_own[...]
    for k in range(len(group)):
        down += dn_peer[k]
    down_norm_ref[...] = down

    gg_copy(1).wait_recv()
    gg_copy(2).wait_recv()
    for step in range(1, n_tp):
        gg_copy(step - 1).wait_send()
        gi_copy(step).wait_send()
    for k in range(len(group)):
        dn_copy(k).wait_send()
    loop(0, blocks, lambda j: y_copy(j).wait_send())

    @pl.when(at_end)
    def _():
        for slot in range(3):
            l_copy(slot).wait_send()
        loop(0, blocks, lambda t: a_copy(t, 0).wait_send())
        loop(0, blocks, lambda t: a_copy(t, 1).wait_send())
        loop(0, 2 * blocks, lambda q: r_copy(q).wait_send())

    @pl.when(jnp.logical_not(at_end))
    def _():
        for slot in range(3):
            for hop in range(3):
                m_copy(slot, hop).wait_send()
        loop(0, blocks, lambda t: b_copy(0, t).wait_send())
        loop(blocks, 3 * blocks, lambda t: b_copy(1, t).wait_send())
        loop(0, 3 * blocks, lambda t: c_copy(t).wait_send())
        loop(0, 2 * blocks, lambda q: f_copy(q).wait_send())

    for step in range(1, n_tp):
        gn_copy(step).wait_recv()
    gate_up = gu_own[...]
    for step in range(1, n_tp):
        gate_up += gu_peer[step - 1]
    gu_norm_ref[...] = gate_up
    for step in range(1, n_tp):
        gn_copy(step).wait_send()


def store_kernel(gi_ref, gate_ref, up_ref, down_ref, gu_ref, dn_ref, *rest):
    sem, outs = rest[-1], rest[:-1]
    owned = gu_ref.shape[1] // 2
    sources = (
        gate_ref, up_ref, down_ref, gi_ref, gu_ref.at[:, pl.ds(0, owned)], gu_ref.at[:, pl.ds(owned, owned)], dn_ref
    )
    copies = [pltpu.make_async_copy(src, dst, sem.at[k]) for k, (src, dst) in enumerate(zip(sources, outs))]
    for copy in copies:
        copy.start()
    for copy in copies:
        copy.wait()


def on_line(inputs, gate_pre, up_pre, cotangent, w_gate, w_up, w_down):
    n_fs, n_tp = lax.axis_size("fs"), lax.axis_size("tp")
    tokens, width = inputs.shape
    hunits = w_gate.shape[1]
    blocks = hunits // LANES
    items = 3 * blocks
    owned = width // 4
    share = tokens // n_tp
    n_group = 4 * n_fs - 1
    dma = pltpu.SemaphoreType.DMA
    vmem = pltpu.VMEM
    sizes = (n_fs, n_tp, float(tokens * 4) ** (-0.5))
    shaped = jax.ShapeDtypeStruct
    gi_shape = shaped((tokens, width), BF16)
    row_shape = shaped((owned, 1, hunits), F32)
    down_shape = shaped((hunits, 1, owned), F32)
    results = pl.pallas_call(
        functools.partial(line_kernel, sizes),
        out_shape=(
            vmem((tokens, width), BF16),
            vmem((owned, 1, hunits), F32),
            vmem((owned, 1, hunits), F32),
            vmem((hunits, 1, owned), F32),
            vmem((1, 2 * owned), F32),
            vmem((1, hunits), F32),
        ),
        in_specs=[pl.BlockSpec(memory_space=pltpu.HBM)] * 7,
        out_specs=(pl.BlockSpec(memory_space=vmem),) * 6,
        scratch_shapes=[
            vmem((tokens, width), BF16),
            vmem((tokens, hunits), BF16),
            vmem((tokens, hunits), BF16),
            vmem((tokens, width), BF16),
            vmem((width, hunits), BF16),
            vmem((width, hunits), BF16),
            vmem((hunits, width), BF16),
            vmem((2, width, tokens), BF16),
            vmem((3 * owned, tokens), BF16),
            vmem((items, tokens, LANES), BF16),
            vmem((2 * blocks, tokens, LANES), BF16),
            vmem((blocks, tokens, LANES), BF16),
            vmem((blocks, tokens, LANES), BF16),
            vmem((blocks, 3 * owned, LANES), BF16),
            vmem((2 * blocks, 2 * owned, LANES), BF16),
            vmem((items, 2 * owned, LANES), BF16),
            vmem((tokens, width), F32),
            vmem((tokens, width), BF16),
            vmem((n_tp - 1, share, width), BF16),
            vmem((2, owned, LANES), F32),
            vmem((1, 2 * owned), F32),
            vmem((n_tp - 1, 1, 2 * owned), F32),
            vmem((1, hunits), F32),
            vmem((n_group, 1, hunits), F32),
            dma((7,)),
            dma((blocks,)), dma((blocks,)),
            dma((2 * blocks,)), dma((2 * blocks,)),
            dma((items,)), dma((items,)),
            dma((items,)), dma((items,)),
            dma((2 * blocks,)), dma((2 * blocks,)),
            dma((2 * blocks,)), dma((2 * blocks,)),
            dma((3,)), dma((3,)),
            dma((9,)), dma((9,)),
            dma((n_tp - 1,)), dma((n_tp - 1,)),
            dma((n_tp - 1,)), dma((n_tp - 1,)),
            dma((n_tp - 1,)), dma((n_tp - 1,)),
            dma((n_group,)), dma((n_group,)),
        ],
        compiler_params=pltpu.CompilerParams(
            collective_id=0, has_side_effects=True, vmem_limit_bytes=VMEM_LIMIT
        ),
    )(inputs, gate_pre, up_pre, cotangent, w_gate, w_up, w_down)
    grad_gate, grad_up, grad_down, grad_input, gate_norms, up_norms, down_norms = pl.pallas_call(
        store_kernel,
        out_shape=(
            row_shape, row_shape, down_shape, gi_shape,
            shaped((1, owned), F32), shaped((1, owned), F32), shaped((1, hunits), F32),
        ),
        in_specs=[pl.BlockSpec(memory_space=vmem)] * 6,
        out_specs=(pl.BlockSpec(memory_space=pltpu.HBM),) * 7,
        scratch_shapes=[dma((7,))],
        compiler_params=pltpu.CompilerParams(vmem_limit_bytes=2**23),
    )(*results)
    return (
        grad_input,
        grad_gate,
        grad_up,
        grad_down.transpose(0, 2, 1),
        gate_norms.reshape(owned, 1),
        up_norms.reshape(owned, 1),
        down_norms.reshape(hunits),
    )


def fits_line(mesh, inputs, w_gate):
    n_rep, n_fs, n_tp = (mesh.shape[axis] for axis in ("rep", "fs", "tp"))
    tokens, width = inputs.shape[0] // n_rep, inputs.shape[1] // n_fs
    return (
        n_rep == 4 and n_fs == 2 and n_tp == 4 and w_gate.shape[1] // n_tp >= 10 * LANES
        and width % (4 * LANES) == 0
        and tokens % (16 * n_tp) == 0 and tokens % LANES == 0
        and (w_gate.shape[1] // n_tp) % LANES == 0
    )


def solution(mesh):
    placed = (
        P("rep", "fs"),
        P("rep", "tp"),
        P("rep", "tp"),
        P("rep", None),
        P("fs", "tp"),
        P("fs", "tp"),
        P("tp", "fs"),
    )
    out_placed = (
        P("rep", "fs"),
        P("fs", "rep", "tp"),
        P("fs", "rep", "tp"),
        P("tp", "fs", "rep"),
        P("fs", "rep"),
        P("fs", "rep"),
        P("tp"),
    )

    def whole(inputs, gate_pre, up_pre, cotangent, w_gate, w_up, w_down):
        body = on_line if fits_line(mesh, inputs, w_gate) else on_device
        mapped = jax.shard_map(body, mesh=mesh, in_specs=placed, out_specs=out_placed, check_vma=False)
        return mapped(inputs, gate_pre, up_pre, cotangent, w_gate, w_up, w_down)

    return whole
```

time: 153 us -> 129 us (0.84)
  Pallas kernels: 142 us -> 127 us
  local copies, waits for them, and re-layouts: 10.1 us -> 0 us
    pallas_call x1 -> x2, Pallas kernels: 142 us -> 127 us  [the longest x1 125 us: on_line(): pl.pallas_call(functools.partial(line_kernel, sizes), out_shape=(vmem((to...]
    unnamed x10 -> x0, local copies, waits for them, and re-layouts: 7.33 us -> none
where the time goes in v1:
time: 129 us; the launch traced here: 128 us
  Pallas kernels  127 us (98%)
    pallas_call x1, Pallas kernels, on_line(): pl.pallas_call(functools.partial(line_kernel, sizes), out_shape=(vmem((to...  125 us

profile of v1, /device:TPU:0, one launch (start us, length us, event | category | flops | bytes accessed | tf_op | source)
XLA Modules:
  0.0 128.5 jit_solution(13802313204237391263)
XLA Ops:
  0.6 124.6 %shard_map.126 = (bf16[640,1024]{1,0:T(8,128)(2,1)S(1)}, f32[256,1,1408]{2,1,0:T(1,128)S(1)}, f32[256,1,1408]{2,1,0:T(1,128)S(1)}, f32[1408,1,256]{2,1,0:T(1,128...) custom-call(bf16[640,1024]{1,0:T(8,128)(2,1)} %x_hbm.1, bf16[640,1408]{1,0:T(8,128)(2,1)} %gate_hbm.1, ...), custom_call_target="tpu_custom_call" | custom-call | tf_op jit(solution)/shard_map/pallas_call | solution.py:581
  125.3 2.6 %shard_map.127 = (f32[256,1,1408]{2,1,0:T(1,128)}, f32[256,1,1408]{2,1,0:T(1,128)}, f32[1408,1,256]{2,1,0:T(1,128)}, bf16[640,1024]{1,0:T(8,128)(2,1)}, f32[1,25...) custom-call(bf16[640,1024]{1,0:T(8,128)(2,1)S(1)} %get-tuple-element.20.gi_ref, ...), custom_call_target="tpu_custom_call" | custom-call | tf_op jit(solution)/shard_map/pallas_call | solution.py:636
  127.8 0.6 reduce

commit v2 on v1

--- a/solution.py
+++ b/solution.py
@@ -10,6 +10,7 @@
 LANES = 128
 CHUNK = 256
 LATE = 4
+AHEAD = 3
 VMEM_LIMIT = 56 * 2**20
 F32 = jnp.float32
 BF16 = jnp.bfloat16
@@ -76,15 +77,18 @@
     gi_ref, gate_out, up_out, down_out, gu_norm_ref, down_norm_ref,
     x_ref, gate_ref, up_ref, cot_ref, wg_ref, wu_ref, wd_ref,
     left, left_far, right, right_far, pg_own, pg_peer, ab, sb, bb, gi_acc, gi_own, gi_peer,
-    squares, gu_own, gu_peer, dn_own, dn_peer,
-    load_sem, y_send, y_recv, a_send, a_recv, b_send, b_recv, c_send, c_recv,
-    r_send, r_recv, f_send, f_recv, l_send, l_recv, m_send, m_recv,
-    gi_send, gi_recv, gg_send, gg_recv, gn_send, gn_recv, dn_send, dn_recv,
+    squares, gu_own, gu_peer, dn_own, dn_peer, dn_sum,
+    load_sem, sends, y_recv, a_recv, bc_recv, d_recv, r_recv, f_recv, l_recv, m_recv, gg_recv, sums_recv, dn_recv,
 ):
     n_fs, n_tp, factor = sizes
+    y_send, a_send, b_send, c_send, r_send, f_send, l_send, m_send, gi_send, gg_send, gn_send, dn_send = (
+        sends.at[k] for k in range(12)
+    )
+    gi_recv, gn_recv = (sums_recv.at[k] for k in range(2))
     tokens, width = x_ref.shape
     hunits = gate_ref.shape[1]
     blocks = hunits // LANES
+    items = 3 * blocks
     owned = width // 4
     share = tokens // n_tp
     rep, fs, tp = lax.axis_index("rep"), lax.axis_index("fs"), lax.axis_index("tp")
@@ -97,30 +101,36 @@
     tp_next = tp + 1 - 2 * lax.rem(tp, 2)
     tp_far = lax.rem(tp + 2, n_tp)
 
+    first = AHEAD * LANES
+    rest = hunits - first
     loads = [
         pltpu.make_async_copy(cot_hbm.at[:, pl.ds(pl.multiple_of(fs * width, LANES), width)], cot_ref, load_sem.at[0]),
-        pltpu.make_async_copy(wd_hbm, wd_ref, load_sem.at[1]),
+        pltpu.make_async_copy(wd_hbm.at[pl.ds(0, first)], wd_ref.at[pl.ds(0, first)], load_sem.at[1]),
         pltpu.make_async_copy(gate_hbm, gate_ref, load_sem.at[2]),
         pltpu.make_async_copy(up_hbm, up_ref, load_sem.at[3]),
         pltpu.make_async_copy(x_hbm, x_ref, load_sem.at[4]),
         pltpu.make_async_copy(wg_hbm, wg_ref, load_sem.at[5]),
         pltpu.make_async_copy(wu_hbm, wu_ref, load_sem.at[6]),
+        pltpu.make_async_copy(wd_hbm.at[pl.ds(first, rest)], wd_ref.at[pl.ds(first, rest)], load_sem.at[7]),
     ]
-    for k in (4, 0, 1, 2, 3, 5, 6):
-        loads[k].start()
-
-    group = [(r, f) for r in range(4) for f in range(n_fs) if r or f]
-
-    def in_group(step):
-        return (lax.rem(rep + step[0], 4), lax.rem(fs + step[1], n_fs), tp)
+
+    def load(*which):
+        for k in which:
+            loads[k].start()
+
+    load(4, 0, 1)
 
     def in_tp(step):
         return (rep, fs, lax.rem(tp + step, n_tp))
 
     barrier = pltpu.get_barrier_semaphore()
-    greeted = [in_group(s) for s in group] + [in_tp(s) for s in range(1, n_tp)]
+    greeted = [(partner, fs, tp), (rep, fs_peer, tp)] + [in_tp(s) for s in range(1, n_tp)]
     for other in greeted:
         pl.semaphore_signal(barrier, inc=1, device_id=other, device_id_type=MESH)
+
+    @pl.when(jnp.logical_not(at_end))
+    def _():
+        pl.semaphore_signal(barrier, inc=1, device_id=(far_mid, fs, tp), device_id_type=MESH)
 
     def remote(src, dst, send, recv, other):
         return pltpu.make_async_remote_copy(
@@ -131,20 +141,25 @@
         return slice(slot * owned, (slot + 1) * owned)
 
     def y_copy(j):
-        return remote(pg_own.at[j], pg_peer.at[j], y_send.at[j], y_recv.at[j], (rep, fs_peer, tp))
+        return remote(pg_own.at[j], pg_peer.at[j], y_send, y_recv.at[j], (rep, fs_peer, tp))
 
     def a_copy(t, late):
         piece = ab.at[t, pl.ds(0, owned) if late else pl.ds(owned, 2 * owned)]
         k = blocks * late + t
-        return remote(piece, piece, a_send.at[k], a_recv.at[k], (partner, fs, tp))
+        return remote(piece, piece, a_send, a_recv.at[k], (partner, fs, tp))
 
     def b_copy(kind, t):
         src = ab.at[t, pl.ds(owned, 2 * owned)] if kind == 0 else sb.at[t - blocks]
-        return remote(src, bb.at[t], b_send.at[t], b_recv.at[t], (far_mid, fs, tp))
+        return remote(src, bb.at[t], b_send, bc_recv.at[t], (far_mid, fs, tp))
+
+    def last_copy(t, slot):
+        rows = pl.ds(slot * owned, owned)
+        recv = d_recv.at[t - items + 4] if slot else bc_recv.at[t]
+        return remote(sb.at[t - blocks, rows], bb.at[t, rows], b_send, recv, (far_mid, fs, tp))
 
     def c_copy(t):
         return remote(
-            bb.at[t, pl.ds(owned, owned)], bb.at[t, pl.ds(0, owned)], c_send.at[t], c_recv.at[t], (partner, fs, tp)
+            bb.at[t, pl.ds(owned, owned)], bb.at[t, pl.ds(0, owned)], c_send, bc_recv.at[t], (partner, fs, tp)
         )
 
     half = tokens // n_fs
@@ -152,12 +167,12 @@
 
     def r_copy(q):
         return remote(
-            right.at[blocks + q, own_half], right_far.at[q, own_half], r_send.at[q], r_recv.at[q], (partner, fs, tp)
+            right.at[blocks + q, own_half], right_far.at[q, own_half], r_send, r_recv.at[q], (partner, fs, tp)
         )
 
     def f_copy(q):
         piece = right_far.at[q, own_half]
-        return remote(piece, piece, f_send.at[q], f_recv.at[q], (rep, fs_peer, tp))
+        return remote(piece, piece, f_send, f_recv.at[q], (rep, fs_peer, tp))
 
     piece_rows = owned // n_tp
 
@@ -166,12 +181,12 @@
 
     def l_copy(slot):
         rows = piece_of(slot, tp)
-        return remote(left.at[1, rows], left_far.at[rows], l_send.at[slot], l_recv.at[slot], (partner, fs, tp))
+        return remote(left.at[1, rows], left_far.at[rows], l_send, l_recv.at[slot], (partner, fs, tp))
 
     def m_copy(slot, hop):
         piece = left_far.at[piece_of(slot, tp_far if hop == 2 else tp)]
         k = 3 * slot + hop
-        return remote(piece, piece, m_send.at[k], m_recv.at[k], (rep, fs, tp_next if hop else tp_far))
+        return remote(piece, piece, m_send, m_recv.at[k], (rep, fs, tp_next if hop else tp_far))
 
     def lanes(j):
         return pl.ds(pl.multiple_of(j * LANES, LANES), LANES)
@@ -268,6 +283,21 @@
         if kind:
             finish(kind, j, long_term(0, 1, t) + bb[t, :owned, :].astype(F32))
 
+    def last_on(t):
+        f_copy(t - blocks).wait_recv()
+        sb[t - blocks] = long_term(1, 3, t).astype(BF16)
+        last_copy(t, 1).start()
+
+    def last_settle(t):
+        last_copy(t, 1).wait_recv()
+        bb[t, owned:, :] = (bb[t, owned:, :].astype(F32) + term(1, 3, 4, t)).astype(BF16)
+        c_copy(t).start()
+
+    def last_own(kind, j):
+        t = item(kind, j)
+        last_copy(t, 0).wait_recv()
+        finish(kind, j, long_term(0, 1, t) + bb[t, :owned, :].astype(F32))
+
     def settle_own(j):
         a_copy(j, 1).wait_recv()
         finish(0, j, ab[j, :owned, :].astype(F32) + term(0, 0, 1, j) + bb[j, :owned, :].astype(F32))
@@ -293,21 +323,28 @@
     def gi_copy(step):
         other = lax.rem(tp + step, n_tp)
         return remote(
-            gi_own.at[tokens_of(other)], gi_peer.at[step - 1], gi_send.at[step - 1], gi_recv.at[step - 1], in_tp(step)
+            gi_own.at[tokens_of(other)], gi_peer.at[step - 1], gi_send, gi_recv, in_tp(step)
         )
 
     def gg_copy(hop):
         piece = gi_ref.at[tokens_of(tp_far if hop == 2 else tp)]
-        return remote(piece, piece, gg_send.at[hop], gg_recv.at[hop], (rep, fs, tp_next if hop else tp_far))
+        return remote(piece, piece, gg_send, gg_recv.at[hop], (rep, fs, tp_next if hop else tp_far))
 
     def gi_out():
         gi_own[...] = gi_acc[...].astype(BF16)
         for step in range(1, n_tp):
             gi_copy(step).start()
 
+    here = (rep, fs_peer, tp)
+
+    def all_in(whole, recv):
+        remote(whole, whole, gi_send, recv, here).wait_recv()
+
+    def all_out(whole, send):
+        remote(whole, whole, send, gi_recv, here).wait_send()
+
     def gi_sum():
-        for step in range(1, n_tp):
-            gi_copy(step).wait_recv()
+        all_in(gi_peer, gi_recv)
         whole = gi_own[tokens_of(tp), :].astype(F32)
         for step in range(1, n_tp):
             whole += gi_peer[step - 1].astype(F32)
@@ -320,30 +357,64 @@
         gg_copy(2).start()
 
     def dn_copy(k):
-        return remote(dn_own, dn_peer.at[k], dn_send.at[k], dn_recv.at[k], in_group(group[k]))
-
-    def dn_out():
-        for k in range(len(group)):
-            dn_copy(k).start()
+        src = dn_sum.at[k] if k < 3 else dn_own
+        place, other = ((1, (rep, fs_peer, tp)), (2, (far_mid, fs, tp)), (0, (partner, fs, tp)), (0, (partner, fs, tp)))[k]
+        return remote(src, dn_peer.at[place], dn_send, dn_recv.at[place], other)
+
+    def dn_on(k):
+        dn_copy((3, 0, 1)[k]).wait_recv()
+        dn_sum[k] = (dn_sum[k - 1] if k else dn_own[...]) + dn_peer[k]
+        dn_copy(k).start()
 
     def gn_copy(step):
-        return remote(gu_own, gu_peer.at[step - 1], gn_send.at[step - 1], gn_recv.at[step - 1], in_tp(step))
+        return remote(gu_own, gu_peer.at[step - 1], gn_send, gn_recv, in_tp(step))
 
     loads[4].wait()
+    load(2, 3)
     spread(1, x_ref)
-    pl.semaphore_wait(barrier, len(greeted))
-
-    @pl.when(at_end)
-    def _():
-        l_copy(1).start()
-        l_copy(2).start()
-
     loads[0].wait()
     loads[1].wait()
-    loop(0, 1, partial_out)
+    load(7)
+    loop(0, 1, partial_of)
+
+    @pl.when(at_end)
+    def _():
+        pl.semaphore_wait(barrier, len(greeted))
+
+    @pl.when(jnp.logical_not(at_end))
+    def _():
+        pl.semaphore_wait(barrier, len(greeted) + 1)
+
+    y_copy(0).start()
+
+    turn = blocks // 2
+
+    def past(j, k):
+        return jnp.where(j > k, 1, 0)
+
+    def down_from(j):
+        return jnp.minimum(j + 1 + past(j, turn) + past(j, turn + 2), blocks)
+
+    def down_to(j):
+        return jnp.minimum(j + 2 + past(j, turn - 1) + past(j, turn + 1), blocks)
+
+    def late_to(j):
+        return jnp.minimum(sum(jnp.maximum(j - LATE + k, 0) for k in (1, -1, -3)), blocks)
+
+    def sent_to(j):
+        return jnp.minimum(j + AHEAD + past(j, 1), blocks)
+
+    def grads_to(j):
+        return jnp.minimum(j + AHEAD + past(j, 3), blocks)
+
+    @pl.when(at_end)
+    def _():
+        l_copy(1).start()
+
     spread(0, cot_ref)
     loads[2].wait()
     loads[3].wait()
+    load(5, 6)
 
     @pl.when(at_end)
     def _():
@@ -357,26 +428,25 @@
             r_copy(2 * j + 1).start()
 
         loop(0, 1, out)
-        loop(1, 6, partial_out)
+        l_copy(2).start()
+        loop(1, AHEAD, partial_out)
+        loads[7].wait()
+        loop(AHEAD, 6, partial_out)
         gi_acc[...] = jnp.zeros_like(gi_acc)
 
         def both_out(j):
             pair_out(j)
-            out(j + 1)
+            loop(down_from(j), down_to(j), out)
 
             @pl.when(j == 1)
             def _():
                 l_copy(0).start()
 
-            @pl.when(j >= LATE)
-            def _():
-                a_copy(j - LATE, 1).start()
+            loop(late_to(j - 1), late_to(j), lambda t: a_copy(t, 1).start())
 
         loop(0, 1, both_out)
         loop(6, blocks, partial_out)
-        loop(1, blocks - 1, both_out)
-        pair_out(blocks - 1)
-        loop(blocks - 1 - LATE, blocks, lambda t: a_copy(t, 1).start())
+        loop(1, blocks, both_out)
         squares[...] = jnp.zeros_like(squares)
         loads[5].wait()
         loads[6].wait()
@@ -384,180 +454,166 @@
         gi_out()
 
         def hops(j):
-            last_hop(0, j - 1)
+            loop(down_from(j - 2), down_to(j - 2), functools.partial(last_hop, 0))
             last_hop(1, j - 2)
             last_hop(2, j - 2)
 
-        last_hop(0, 0)
+        loop(0, 1, functools.partial(last_hop, 0))
         loop(2, blocks - 3, hops)
         gi_sum()
-        loop(blocks - 3, blocks, hops)
-        last_hop(0, blocks - 1)
-        dn_out()
+        loop(blocks - 3, blocks - 1, hops)
+        dn_copy(3).start()
         gi_pass()
-        for j in (blocks - 2, blocks - 1):
-            last_hop(1, j)
-            last_hop(2, j)
+        loop(blocks - 1, blocks, hops)
+        last_hop(1, blocks - 2)
+        last_hop(2, blocks - 2)
+        last_hop(1, blocks - 1)
+        last_hop(2, blocks - 1)
 
     @pl.when(jnp.logical_not(at_end))
     def _():
-        loop(1, 2, partial_out)
-        loop(2, 6, partial_of)
-        for slot in (1, 2):
+        def spread_on(slot):
             l_copy(slot).wait_recv()
             m_copy(slot, 0).start()
             m_copy(slot, 1).start()
-        loop(6, blocks, partial_of)
+
+        def pass_on(slot):
+            m_copy(slot, 0).wait_recv()
+            m_copy(slot, 2).start()
+
+        def landed(slot):
+            m_copy(slot, 1).wait_recv()
+            m_copy(slot, 2).wait_recv()
+
+        def feed(j):
+            forward(2 * j)
+            forward(2 * j + 1)
+
+            loop(sent_to(j - 1), sent_to(j), lambda k: y_copy(k).start())
+
+        loop(1, 2, partial_out)
+        loop(2, AHEAD, partial_of)
+        loads[7].wait()
+        loop(AHEAD, 8, partial_of)
+        spread_on(1)
+        loop(8, blocks, partial_of)
         loop(0, blocks, hidden_of)
         down_on(0)
         grads_of(0)
-        for slot in (1, 2):
-            m_copy(slot, 0).wait_recv()
-            m_copy(slot, 2).start()
-        forward(0)
+        spread_on(2)
+        pass_on(1)
         gi_acc[...] = jnp.zeros_like(gi_acc)
         squares[...] = jnp.zeros_like(squares)
+        feed(0)
+        pass_on(2)
         loads[5].wait()
         loads[6].wait()
-        forward(1)
-        y_copy(2).start()
-        for slot in (1, 2):
-            m_copy(slot, 1).wait_recv()
-            m_copy(slot, 2).wait_recv()
-        pair_on(1, 0)
-        down_on(1)
-        pair_on(2, 0)
-        grads_and_term(1)
-
-        def first_y(j):
-            return j + 2 + jnp.where(j > 3, 1, 0) + jnp.where(j > 5, 1, 0)
-
-        def step(j, late):
-            forward(2 * j)
-            forward(2 * j + 1)
-            if not late:
-                new, old = first_y(j), first_y(j - 1)
-                for extra in range(2):
-                    @pl.when(jnp.logical_and(new + extra < blocks, extra == 0 if extra == 0 else jnp.logical_or(j == 3, j == 5)))
-                    def _():
-                        y_copy(new + extra).start()
-                for extra in range(2):
-                    @pl.when(jnp.logical_and(old + extra < blocks, extra == 0 if extra == 0 else jnp.logical_or(j == 4, j == 6)))
-                    def _():
-                        grads_and_term(old + extra)
+        landed(1)
+        landed(2)
+
+        def step(j):
             pair_on(1, j)
+            loop(down_from(j), down_to(j), down_on)
             pair_on(2, j)
 
-        def early_step(j):
-            step(j, False)
-            down_on(j + 1)
-
-        loop(1, 2, early_step)
-        gi_term(0)
-        l_copy(0).wait_recv()
-        m_copy(0, 0).start()
-        m_copy(0, 1).start()
-        settle(0, 0)
-        m_copy(0, 0).wait_recv()
-        m_copy(0, 2).start()
+            @pl.when(j + 1 < blocks)
+            def _():
+                feed(j + 1)
+
+            @pl.when(j == 0)
+            def _():
+                gi_term(0)
+                grads_and_term(1)
+
+            loop(grads_to(j - 1), grads_to(j), grads_and_term)
 
         def settles(j):
-            settle(0, j - 1)
+            loop(down_from(j - 2), down_to(j - 2), functools.partial(settle, 0))
             settle(1, j - 2)
             settle(2, j - 2)
-
-            @pl.when(j >= LATE + 1)
-            def _():
-                settle_own(j - LATE - 1)
-
-        loop(2, 3, early_step)
-        m_copy(0, 1).wait_recv()
-        m_copy(0, 2).wait_recv()
+            loop(late_to(j - 2), late_to(j - 1), settle_own)
+
+        loop(0, 2, step)
+        spread_on(0)
+        loop(0, 1, functools.partial(settle, 0))
+        pass_on(0)
+        step(2)
+        landed(0)
 
         def both(j):
             settles(j - 1)
-            early_step(j)
+            step(j)
 
         loop(3, blocks - 3, both)
         gi_out()
-
-        def late_both(j):
-            settles(j - 1)
-            step(j, True)
-            down_on(j + 1)
-
-        loop(blocks - 3, blocks - 1, late_both)
+        loop(blocks - 3, blocks - 2, both)
+        settles(blocks - 3)
+        loop(items - 4, items - 2, last_on)
+        feed(blocks - 1)
         gi_sum()
         settles(blocks - 2)
-        step(blocks - 1, True)
+        loop(items - 2, items, last_on)
+        loop(items - 4, items, lambda t: last_copy(t, 0).start())
         settles(blocks - 1)
         gi_pass()
-        loop(blocks - 1 - LATE, blocks - 1, settle_own)
-        settle(0, blocks - 1)
-        settle_own(blocks - 1)
-        dn_out()
+        dn_on(0)
+        loop(items - 4, items, last_settle)
+        dn_on(1)
         for j in (blocks - 2, blocks - 1):
-            settle(1, j)
-            settle(2, j)
+            last_own(1, j)
+            last_own(2, j)
+        dn_on(2)
+        down_norm_ref[...] = dn_sum[2]
 
     for kind in range(2):
         gu_own[0:1, kind * owned:(kind + 1) * owned] = jnp.sum(squares[kind].T, axis=0, keepdims=True)
     for step in range(1, n_tp):
         gn_copy(step).start()
 
-    for k in range(len(group)):
-        dn_copy(k).wait_recv()
-    down = dn_own[...]
-    for k in range(len(group)):
-        down += dn_peer[k]
-    down_norm_ref[...] = down
+    @pl.when(at_end)
+    def _():
+        dn_copy(2).wait_recv()
+        down_norm_ref[...] = dn_peer[0]
 
     gg_copy(1).wait_recv()
     gg_copy(2).wait_recv()
-    for step in range(1, n_tp):
-        gg_copy(step - 1).wait_send()
-        gi_copy(step).wait_send()
-    for k in range(len(group)):
-        dn_copy(k).wait_send()
-    loop(0, blocks, lambda j: y_copy(j).wait_send())
+    all_out(gi_peer, gi_send)
+    all_out(gi_ref.at[pl.ds(0, 3 * share)], gg_send)
+    all_out(pg_peer, y_send)
 
     @pl.when(at_end)
     def _():
-        for slot in range(3):
-            l_copy(slot).wait_send()
-        loop(0, blocks, lambda t: a_copy(t, 0).wait_send())
-        loop(0, blocks, lambda t: a_copy(t, 1).wait_send())
-        loop(0, 2 * blocks, lambda q: r_copy(q).wait_send())
+        all_out(left_far.at[pl.ds(0, 3 * piece_rows)], l_send)
+        all_out(ab, a_send)
+        all_out(dn_own, dn_send)
+        all_out(right_far.at[:, own_half], r_send)
 
     @pl.when(jnp.logical_not(at_end))
     def _():
-        for slot in range(3):
-            for hop in range(3):
-                m_copy(slot, hop).wait_send()
-        loop(0, blocks, lambda t: b_copy(0, t).wait_send())
-        loop(blocks, 3 * blocks, lambda t: b_copy(1, t).wait_send())
-        loop(0, 3 * blocks, lambda t: c_copy(t).wait_send())
-        loop(0, 2 * blocks, lambda q: f_copy(q).wait_send())
-
-    for step in range(1, n_tp):
-        gn_copy(step).wait_recv()
+        all_out(left_far.at[pl.ds(0, 9 * piece_rows)], m_send)
+        all_out(bb, b_send)
+        all_out(dn_sum, dn_send)
+        all_out(bb.at[:, pl.ds(0, owned)], c_send)
+        all_out(right_far.at[:, own_half], f_send)
+
+    all_in(gu_peer, gn_recv)
     gate_up = gu_own[...]
     for step in range(1, n_tp):
         gate_up += gu_peer[step - 1]
     gu_norm_ref[...] = gate_up
-    for step in range(1, n_tp):
-        gn_copy(step).wait_send()
+    all_out(gu_peer, gn_send)
 
 
 def store_kernel(gi_ref, gate_ref, up_ref, down_ref, gu_ref, dn_ref, *rest):
-    sem, outs = rest[-1], rest[:-1]
+    sem, line, outs = rest[-1], rest[-2], rest[:-2]
     owned = gu_ref.shape[1] // 2
     sources = (
-        gate_ref, up_ref, down_ref, gi_ref, gu_ref.at[:, pl.ds(0, owned)], gu_ref.at[:, pl.ds(owned, owned)], dn_ref
+        gate_ref, up_ref, down_ref, gi_ref, gu_ref.at[:, pl.ds(0, owned)], gu_ref.at[:, pl.ds(owned, owned)]
     )
     copies = [pltpu.make_async_copy(src, dst, sem.at[k]) for k, (src, dst) in enumerate(zip(sources, outs))]
     for copy in copies:
         copy.start()
+    line[...] = dn_ref[0, :]
     for copy in copies:
         copy.wait()
 
@@ -570,7 +626,6 @@
     items = 3 * blocks
     owned = width // 4
     share = tokens // n_tp
-    n_group = 4 * n_fs - 1
     dma = pltpu.SemaphoreType.DMA
     vmem = pltpu.VMEM
     sizes = (n_fs, n_tp, float(tokens * 4) ** (-0.5))
@@ -614,20 +669,21 @@
             vmem((1, 2 * owned), F32),
             vmem((n_tp - 1, 1, 2 * owned), F32),
             vmem((1, hunits), F32),
-            vmem((n_group, 1, hunits), F32),
-            dma((7,)),
-            dma((blocks,)), dma((blocks,)),
-            dma((2 * blocks,)), dma((2 * blocks,)),
-            dma((items,)), dma((items,)),
-            dma((items,)), dma((items,)),
-            dma((2 * blocks,)), dma((2 * blocks,)),
-            dma((2 * blocks,)), dma((2 * blocks,)),
-            dma((3,)), dma((3,)),
-            dma((9,)), dma((9,)),
-            dma((n_tp - 1,)), dma((n_tp - 1,)),
-            dma((n_tp - 1,)), dma((n_tp - 1,)),
-            dma((n_tp - 1,)), dma((n_tp - 1,)),
-            dma((n_group,)), dma((n_group,)),
+            vmem((3, 1, hunits), F32),
+            vmem((3, 1, hunits), F32),
+            dma((8,)),
+            dma((12,)),
+            dma((blocks,)),
+            dma((2 * blocks,)),
+            dma((items,)),
+            dma((4,)),
+            dma((2 * blocks,)),
+            dma((2 * blocks,)),
+            dma((3,)),
+            dma((9,)),
+            dma((3,)),
+            dma((2,)),
+            dma((3,)),
         ],
         compiler_params=pltpu.CompilerParams(
             collective_id=0, has_side_effects=True, vmem_limit_bytes=VMEM_LIMIT
@@ -637,11 +693,11 @@
         store_kernel,
         out_shape=(
             row_shape, row_shape, down_shape, gi_shape,
-            shaped((1, owned), F32), shaped((1, owned), F32), shaped((1, hunits), F32),
+            shaped((1, owned), F32), shaped((1, owned), F32), shaped((hunits,), F32),
         ),
         in_specs=[pl.BlockSpec(memory_space=vmem)] * 6,
-        out_specs=(pl.BlockSpec(memory_space=pltpu.HBM),) * 7,
-        scratch_shapes=[dma((7,))],
+        out_specs=(pl.BlockSpec(memory_space=pltpu.HBM),) * 6 + (pl.BlockSpec(memory_space=vmem),),
+        scratch_shapes=[dma((6,))],
         compiler_params=pltpu.CompilerParams(vmem_limit_bytes=2**23),
     )(*results)
     return (
@@ -651,7 +707,7 @@
         grad_down.transpose(0, 2, 1),
         gate_norms.reshape(owned, 1),
         up_norms.reshape(owned, 1),
-        down_norms.reshape(hunits),
+        down_norms,
     )
 
 

time: 129 us -> 123 us (0.953)
  Pallas kernels: 127 us -> 121 us
    pallas_call x1, Pallas kernels: 125 us -> 118 us  [on_line(): pl.pallas_call(functools.partial(line_kernel, sizes), out_shape=(vmem((to...]
where the time goes in v2:
time: 123 us; the launch traced here: 122 us
  Pallas kernels  121 us (98%)
    pallas_call x1, Pallas kernels, on_line(): pl.pallas_call(functools.partial(line_kernel, sizes), out_shape=(vmem((to...  118 us
    pallas_call x1, Pallas kernels, on_line(): pl.pallas_call(store_kernel, out_shape=(row_shape, row_shape, down_shape,...  3.13 us

profile of v2, /device:TPU:0, one launch (start us, length us, event | category | flops | bytes accessed | tf_op | source)
XLA Modules:
  0.0 122.2 jit_solution(629223723264447203)
XLA Ops:
  0.6 118.2 %shard_map.126 = (bf16[640,1024]{1,0:T(8,128)(2,1)S(1)}, f32[256,1,1408]{2,1,0:T(1,128)S(1)}, f32[256,1,1408]{2,1,0:T(1,128)S(1)}, f32[1408,1,256]{2,1,0:T(1,128...) custom-call(bf16[640,1024]{1,0:T(8,128)(2,1)} %x_hbm.1, bf16[640,1408]{1,0:T(8,128)(2,1)} %gate_hbm.1, ...), custom_call_target="tpu_custom_call" | custom-call | tf_op jit(solution)/shard_map/pallas_call | solution.py:636
  118.9 3.1 %shard_map.127 = (f32[256,1,1408]{2,1,0:T(1,128)}, f32[256,1,1408]{2,1,0:T(1,128)}, f32[1408,1,256]{2,1,0:T(1,128)}, bf16[640,1024]{1,0:T(8,128)(2,1)}, f32[1,25...) custom-call(bf16[640,1024]{1,0:T(8,128)(2,1)S(1)} %get-tuple-element.20.gi_ref, ...), custom_call_target="tpu_custom_call" | custom-call | tf_op jit(solution)/shard_map/pallas_call | solution.py:692

commit v3 on v2

--- a/solution.py
+++ b/solution.py
@@ -165,6 +165,27 @@
     half = tokens // n_fs
     own_half = pl.ds(pl.multiple_of(fs * half, 16), half)
 
+    peer_half = pl.ds(pl.multiple_of(fs_peer * half, 16), half)
+
+    def y_half(part):
+        rows = own_half if part else peer_half
+        return remote(
+            pg_own.at[0, rows], pg_peer.at[0, rows], y_send, y_recv.at[blocks * part], (rep, fs_peer, tp)
+        )
+
+    def quarter_of(part):
+        return pl.ds(pl.multiple_of(fs * half + part * (half // 2), 16), half // 2)
+
+    def r_first(part):
+        rows = quarter_of(part)
+        return remote(
+            right.at[blocks, rows], right_far.at[0, rows], r_send, r_recv.at[2 * blocks * part], (partner, fs, tp)
+        )
+
+    def f_first(part):
+        piece = right_far.at[0, quarter_of(part)]
+        return remote(piece, piece, f_send, f_recv.at[0], (rep, fs_peer, tp))
+
     def r_copy(q):
         return remote(
             right.at[blocks + q, own_half], right_far.at[q, own_half], r_send, r_recv.at[q], (partner, fs, tp)
@@ -241,15 +262,18 @@
         partial_of(j)
         y_copy(j).start()
 
+    def grads_rows(j, rows):
+        g = gate_ref[rows, lanes(j)].astype(F32)
+        u = up_ref[rows, lanes(j)].astype(F32)
+        total = pg_own[j, rows, :].astype(F32) + pg_peer[j, rows, :].astype(F32)
+        s = 1.0 / (1.0 + jnp.exp(-g))
+        t = blocks + 2 * j
+        right[t, rows, :] = (total * u * s * (1.0 + g * (1.0 - s))).astype(BF16)
+        right[t + 1, rows, :] = (total * (g * s)).astype(BF16)
+
     def grads_of(j):
         y_copy(j).wait_recv()
-        g = gate_ref[:, lanes(j)].astype(F32)
-        u = up_ref[:, lanes(j)].astype(F32)
-        total = pg_own[j].astype(F32) + pg_peer[j].astype(F32)
-        s = 1.0 / (1.0 + jnp.exp(-g))
-        t = blocks + 2 * j
-        right[t] = (total * u * s * (1.0 + g * (1.0 - s))).astype(BF16)
-        right[t + 1] = (total * (g * s)).astype(BF16)
+        grads_rows(j, slice(0, tokens))
 
     def finish(kind, j, piece):
         if kind == 0:
@@ -372,6 +396,17 @@
     loads[4].wait()
     load(2, 3)
     spread(1, x_ref)
+
+    @pl.when(at_end)
+    def _():
+        pl.semaphore_wait(barrier, len(greeted))
+        l_copy(1).start()
+        l_copy(2).start()
+
+    @pl.when(jnp.logical_not(at_end))
+    def _():
+        pl.semaphore_wait(barrier, len(greeted) + 1)
+
     loads[0].wait()
     loads[1].wait()
     load(7)
@@ -379,13 +414,12 @@
 
     @pl.when(at_end)
     def _():
-        pl.semaphore_wait(barrier, len(greeted))
+        y_half(0).start()
+        y_half(1).start()
 
     @pl.when(jnp.logical_not(at_end))
     def _():
-        pl.semaphore_wait(barrier, len(greeted) + 1)
-
-    y_copy(0).start()
+        y_copy(0).start()
 
     turn = blocks // 2
 
@@ -406,10 +440,6 @@
 
     def grads_to(j):
         return jnp.minimum(j + AHEAD + past(j, 3), blocks)
-
-    @pl.when(at_end)
-    def _():
-        l_copy(1).start()
 
     spread(0, cot_ref)
     loads[2].wait()
@@ -428,7 +458,6 @@
             r_copy(2 * j + 1).start()
 
         loop(0, 1, out)
-        l_copy(2).start()
         loop(1, AHEAD, partial_out)
         loads[7].wait()
         loop(AHEAD, 6, partial_out)
@@ -444,7 +473,14 @@
 
             loop(late_to(j - 1), late_to(j), lambda t: a_copy(t, 1).start())
 
-        loop(0, 1, both_out)
+        y_half(0).wait_recv()
+        grads_rows(0, own_half)
+        r_first(0).start()
+        r_first(1).start()
+        r_copy(1).start()
+        out(1)
+        y_half(1).wait_recv()
+        grads_rows(0, peer_half)
         loop(6, blocks, partial_out)
         loop(1, blocks, both_out)
         squares[...] = jnp.zeros_like(squares)
@@ -504,7 +540,11 @@
         pass_on(1)
         gi_acc[...] = jnp.zeros_like(gi_acc)
         squares[...] = jnp.zeros_like(squares)
-        feed(0)
+        for part in range(2):
+            r_first(part).wait_recv()
+            f_first(part).start()
+        forward(1)
+        loop(2, sent_to(0), lambda k: y_copy(k).start())
         pass_on(2)
         loads[5].wait()
         loads[6].wait()
@@ -555,13 +595,17 @@
         loop(items - 2, items, last_on)
         loop(items - 4, items, lambda t: last_copy(t, 0).start())
         settles(blocks - 1)
+        loop(items - 4, items, last_settle)
         gi_pass()
         dn_on(0)
-        loop(items - 4, items, last_settle)
-        dn_on(1)
-        for j in (blocks - 2, blocks - 1):
+
+        def owns(j):
             last_own(1, j)
             last_own(2, j)
+
+        loop(blocks - 2, blocks - 1, owns)
+        dn_on(1)
+        loop(blocks - 1, blocks, owns)
         dn_on(2)
         down_norm_ref[...] = dn_sum[2]
 
@@ -673,11 +717,11 @@
             vmem((3, 1, hunits), F32),
             dma((8,)),
             dma((12,)),
-            dma((blocks,)),
+            dma((blocks + 1,)),
             dma((2 * blocks,)),
             dma((items,)),
             dma((4,)),
-            dma((2 * blocks,)),
+            dma((2 * blocks + 1,)),
             dma((2 * blocks,)),
             dma((3,)),
             dma((9,)),
@@ -717,7 +761,7 @@
     return (
         n_rep == 4 and n_fs == 2 and n_tp == 4 and w_gate.shape[1] // n_tp >= 10 * LANES
         and width % (4 * LANES) == 0
-        and tokens % (16 * n_tp) == 0 and tokens % LANES == 0
+        and tokens % (64 * n_fs) == 0 and tokens % LANES == 0
         and (w_gate.shape[1] // n_tp) % LANES == 0
     )
 

time: 123 us -> 121 us (0.984)
    pallas_call x1, Pallas kernels: 118 us -> 117 us  [on_line(): pl.pallas_call(functools.partial(line_kernel, sizes), out_shape=(vmem((to...]
where the time goes in v3:
time: 121 us
  Pallas kernels  120 us (99%)
    pallas_call x1, Pallas kernels, on_line(): pl.pallas_call(functools.partial(line_kernel, sizes), out_shape=(vmem((to...  117 us
    pallas_call x1, Pallas kernels, on_line(): pl.pallas_call(store_kernel, out_shape=(row_shape, row_shape, down_shape,...  3.13 us

profile of v3, /device:TPU:0, one launch (start us, length us, event | category | flops | bytes accessed | tf_op | source)
XLA Modules:
  0.0 120.5 jit_solution(9741992171891729260)
XLA Ops:
  0.6 116.6 %shard_map.126 = (bf16[640,1024]{1,0:T(8,128)(2,1)S(1)}, f32[256,1,1408]{2,1,0:T(1,128)S(1)}, f32[256,1,1408]{2,1,0:T(1,128)S(1)}, f32[1408,1,256]{2,1,0:T(1,128...) custom-call(bf16[640,1024]{1,0:T(8,128)(2,1)} %x_hbm.1, bf16[640,1408]{1,0:T(8,128)(2,1)} %gate_hbm.1, ...), custom_call_target="tpu_custom_call" | custom-call | tf_op jit(solution)/shard_map/pallas_call | solution.py:680
  117.2 3.1 %shard_map.127 = (f32[256,1,1408]{2,1,0:T(1,128)}, f32[256,1,1408]{2,1,0:T(1,128)}, f32[1408,1,256]{2,1,0:T(1,128)}, bf16[640,1024]{1,0:T(8,128)(2,1)}, f32[1,25...) custom-call(bf16[640,1024]{1,0:T(8,128)(2,1)S(1)} %get-tuple-element.20.gi_ref, ...), custom_call_target="tpu_custom_call" | custom-call | tf_op jit(solution)/shard_map/pallas_call | solution.py:736

commit v4 on v3

--- a/solution.py
+++ b/solution.py
@@ -9,7 +9,7 @@
 
 LANES = 128
 CHUNK = 256
-LATE = 4
+LATE = 6
 AHEAD = 3
 VMEM_LIMIT = 56 * 2**20
 F32 = jnp.float32
@@ -393,6 +393,12 @@
     def gn_copy(step):
         return remote(gu_own, gu_peer.at[step - 1], gn_send, gn_recv, in_tp(step))
 
+    def gn_out():
+        for kind in range(2):
+            gu_own[0:1, kind * owned:(kind + 1) * owned] = jnp.sum(squares[kind].T, axis=0, keepdims=True)
+        for step in range(1, n_tp):
+            gn_copy(step).start()
+
     loads[4].wait()
     load(2, 3)
     spread(1, x_ref)
@@ -433,7 +439,7 @@
         return jnp.minimum(j + 2 + past(j, turn - 1) + past(j, turn + 1), blocks)
 
     def late_to(j):
-        return jnp.minimum(sum(jnp.maximum(j - LATE + k, 0) for k in (1, -1, -3)), blocks)
+        return jnp.minimum(sum(jnp.maximum(j - LATE + k, 0) for k in (1, -1, -2, -3)), blocks)
 
     def sent_to(j):
         return jnp.minimum(j + AHEAD + past(j, 1), blocks)
@@ -483,6 +489,7 @@
         grads_rows(0, peer_half)
         loop(6, blocks, partial_out)
         loop(1, blocks, both_out)
+        loop(late_to(blocks - 1), blocks, lambda t: a_copy(t, 1).start())
         squares[...] = jnp.zeros_like(squares)
         loads[5].wait()
         loads[6].wait()
@@ -495,16 +502,18 @@
             last_hop(2, j - 2)
 
         loop(0, 1, functools.partial(last_hop, 0))
+        def pair_hops(j):
+            last_hop(1, j)
+            last_hop(2, j)
+
         loop(2, blocks - 3, hops)
         gi_sum()
-        loop(blocks - 3, blocks - 1, hops)
+        loop(down_from(blocks - 5), blocks, functools.partial(last_hop, 0))
         dn_copy(3).start()
+        loop(blocks - 5, blocks - 3, pair_hops)
         gi_pass()
-        loop(blocks - 1, blocks, hops)
-        last_hop(1, blocks - 2)
-        last_hop(2, blocks - 2)
-        last_hop(1, blocks - 1)
-        last_hop(2, blocks - 1)
+        loop(blocks - 3, blocks, pair_hops)
+        gn_out()
 
     @pl.when(jnp.logical_not(at_end))
     def _():
@@ -586,33 +595,37 @@
 
         loop(3, blocks - 3, both)
         gi_out()
-        loop(blocks - 3, blocks - 2, both)
-        settles(blocks - 3)
-        loop(items - 4, items - 2, last_on)
-        feed(blocks - 1)
-        gi_sum()
-        settles(blocks - 2)
-        loop(items - 2, items, last_on)
-        loop(items - 4, items, lambda t: last_copy(t, 0).start())
-        settles(blocks - 1)
-        loop(items - 4, items, last_settle)
-        gi_pass()
-        dn_on(0)
+        def pairs(j):
+            settle(1, j)
+            settle(2, j)
 
         def owns(j):
             last_own(1, j)
             last_own(2, j)
 
+        loop(blocks - 3, blocks - 2, both)
+        loop(items - 4, items - 2, last_on)
+        feed(blocks - 1)
+        loop(down_from(blocks - 5), blocks, functools.partial(settle, 0))
+        loop(items - 2, items, last_on)
+        loop(items - 4, items - 2, lambda t: last_copy(t, 0).start())
+        loop(blocks - 5, blocks - 4, pairs)
+        gi_sum()
+        loop(blocks - 4, blocks - 3, pairs)
+        loop(late_to(blocks - 5), blocks - 4, settle_own)
+        loop(blocks - 3, blocks - 2, pairs)
+        loop(blocks - 4, blocks, settle_own)
+        loop(items - 4, items - 2, last_settle)
+        dn_on(0)
+        loop(items - 2, items, last_settle)
+        gi_pass()
+        dn_on(1)
+        loop(items - 2, items, lambda t: last_copy(t, 0).start())
         loop(blocks - 2, blocks - 1, owns)
-        dn_on(1)
+        dn_on(2)
         loop(blocks - 1, blocks, owns)
-        dn_on(2)
+        gn_out()
         down_norm_ref[...] = dn_sum[2]
-
-    for kind in range(2):
-        gu_own[0:1, kind * owned:(kind + 1) * owned] = jnp.sum(squares[kind].T, axis=0, keepdims=True)
-    for step in range(1, n_tp):
-        gn_copy(step).start()
 
     @pl.when(at_end)
     def _():

time: 121 us -> 120 us (level)
  no operation moved by 1% of the time
where the time goes in v4:
time: 120 us
  Pallas kernels  119 us (99%)
    pallas_call x1, Pallas kernels, on_line(): pl.pallas_call(functools.partial(line_kernel, sizes), out_shape=(vmem((to...  116 us
    pallas_call x1, Pallas kernels, on_line(): pl.pallas_call(store_kernel, out_shape=(row_shape, row_shape, down_shape,...  3.13 us

profile of v4, /device:TPU:0, one launch (start us, length us, event | category | flops | bytes accessed | tf_op | source)
XLA Modules:
  0.0 119.7 jit_solution(1602721571282439394)
XLA Ops:
  0.6 115.7 %shard_map.126 = (bf16[640,1024]{1,0:T(8,128)(2,1)S(1)}, f32[256,1,1408]{2,1,0:T(1,128)S(1)}, f32[256,1,1408]{2,1,0:T(1,128)S(1)}, f32[1408,1,256]{2,1,0:T(1,128...) custom-call(bf16[640,1024]{1,0:T(8,128)(2,1)} %x_hbm.1, bf16[640,1408]{1,0:T(8,128)(2,1)} %gate_hbm.1, ...), custom_call_target="tpu_custom_call" | custom-call | tf_op jit(solution)/shard_map/pallas_call | solution.py:693
  116.4 3.1 %shard_map.127 = (f32[256,1,1408]{2,1,0:T(1,128)}, f32[256,1,1408]{2,1,0:T(1,128)}, f32[1408,1,256]{2,1,0:T(1,128)}, bf16[640,1024]{1,0:T(8,128)(2,1)}, f32[1,25...) custom-call(bf16[640,1024]{1,0:T(8,128)(2,1)S(1)} %get-tuple-element.20.gi_ref, ...), custom_call_target="tpu_custom_call" | custom-call | tf_op jit(solution)/shard_map/pallas_call | solution.py:749
